TPU v7x, 32 devices: a whole 2x2x4 slice. The times are simulated.
32 devices in a mesh: sp: 8 (over z, x), tp: 4 (over y, core).
Axes of the slice: x: 2, y: 2, z: 4, core: 2. Of those that a mesh axis runs over, the one named last changes fastest.
Arguments:
- residual: bfloat16 [4096, 2048], P('sp'), may hold values from -6 to 6
- queries: bfloat16 [4096, 1024], P('sp', 'tp'), may hold values from -384 to 384
- key_pairs: bfloat16 [4096, 1024], P('sp', 'tp'), may hold values from -384 to 384
- values: bfloat16 [4096, 1024], P('sp', 'tp'), may hold values from -6 to 6
- lambdas: float32 [8], P('tp'), may hold values from 0.3 to 0.8
- head_gain: float32 [128], replicated, may hold values from 0.1 to 1.9
- w_out: bfloat16 [1024, 2048], replicated, may hold values from -0.1875 to 0.1875
- norm_gain: float32 [2048], replicated, may hold values from 0.1 to 1.9
- w_gate: bfloat16 [2048, 5632], P('sp', 'tp'), may hold values from -0.125 to 0.125
- w_up: bfloat16 [2048, 5632], P('sp', 'tp'), may hold values from -0.125 to 0.125
- w_down: bfloat16 [5632, 2048], P('tp', 'sp'), may hold values from -0.078125 to 0.078125
Outputs:
- layer_out: bfloat16 [4096, 2048], P(('sp', 'tp'))
All inputs are finite; a program needn't handle non-finite values.
Results may differ from a plain program's by a relative error of at most 0.018.
Values may be sent and summed in bfloat16 or wider, within the bound.
A program may use at most 128 MiB of HBM per device.

v0:
```python
import functools

import jax
import jax.numpy as jnp
import numpy as np
from jax import lax
from jax.experimental import pallas as pl
from jax.experimental.pallas import tpu as pltpu
from jax.sharding import Mesh, PartitionSpec as P

HD = 64


def attend_chunk(q, k, v, m_ref, l_ref, acc_ref, slot, rows):
    scores = lax.dot_general(
        q, k, (((1,), (1,)), ((), ())), preferred_element_type=jnp.float32
    )
    old = m_ref[slot, rows, :]
    high = jnp.maximum(old, jnp.max(scores, axis=1, keepdims=True))
    shrink = jnp.exp(old - high)
    weights = jnp.exp(scores - high[:, :1])
    l_ref[slot, rows, :] = l_ref[slot, rows, :] * shrink + jnp.sum(weights, axis=1, keepdims=True)
    m_ref[slot, rows, :] = high
    acc_ref[slot, rows, :] = acc_ref[slot, rows, :] * shrink + jnp.dot(
        weights.astype(jnp.bfloat16), v, preferred_element_type=jnp.float32
    )


def finish_heads(heads, width, lam_ref, gain_ref, l_ref, acc_ref, out_ref):
    for h in range(heads):
        first = acc_ref[2 * h] / l_ref[2 * h]
        second = acc_ref[2 * h + 1] / l_ref[2 * h + 1]
        differ = first - lam_ref[h] * second
        scale = lax.rsqrt(jnp.mean(differ * differ, axis=1, keepdims=True) + 1e-05)
        out_ref[:, h * width : (h + 1) * width] = (differ * scale * gain_ref[...]).astype(out_ref.dtype)


def nearest(k, me, n):
    low, high = me, n - 1 - me
    edge = jnp.minimum(low, high)
    side = jnp.where(high >= low, 1, -1)
    near = jnp.where(k % 2 == 1, 1, -1) * ((k + 1) // 2)
    off = side * jnp.where(k <= 2 * edge, near, k - edge)
    return me + off, off


def gather_attend_kernel(
    nz, nx, heads, block,
    lam_ref, q_ref, kv_ref, gain_ref, pair_ref, down_ref,
    out_ref, pair_out, down_out,
    kv_all, m_ref, l_ref, acc_ref,
    up_sem, low_sem, side_sem, kv_sem, pz_sem, dz_sem, px_sem, dx_sem, p_sem, d_sem,
):
    z, x = lax.axis_index("z"), lax.axis_index("x")
    rows_all = q_ref.shape[0]
    width = out_ref.shape[1] // heads
    keys = heads * 2 * HD
    depth = pair_ref.shape[2]

    def remote(src, dst, send, recv, zz, xx):
        return pltpu.make_async_remote_copy(
            src_ref=src, dst_ref=dst, send_sem=send, recv_sem=recv,
            device_id={"z": zz, "x": xx}, device_id_type=pl.DeviceIdType.MESH,
        )

    barrier = pltpu.get_barrier_semaphore()
    for a in range(nz):
        for b in range(nx):
            if a + b > 0:
                pl.semaphore_signal(
                    barrier, inc=1,
                    device_id={"z": lax.rem(z + a, nz), "x": lax.rem(x + b, nx)},
                    device_id_type=pl.DeviceIdType.MESH,
                )
    pl.semaphore_wait(barrier, nz * nx - 1)

    def slot(zz, xx):
        return zz * nx + xx

    def flow(src, k, zz, go):
        off = zz - z
        here = kv_all.at[slot(zz, x)]

        @pl.when(jnp.logical_and(off <= 0, z < nz - 1))
        def _():
            go(remote(src, here, up_sem.at[k], kv_sem.at[slot(zz, x)], jnp.minimum(z + 1, nz - 1), x))

        @pl.when(jnp.logical_and(off >= 0, z > 0))
        def _():
            go(remote(src, here, low_sem.at[k], kv_sem.at[slot(zz, x)], jnp.maximum(z - 1, 0), x))

        for e in range(1, nx):
            go(remote(src, here, side_sem.at[e - 1, k], kv_sem.at[slot(zz, x)], z, lax.rem(x + e, nx)))

    def pair_place(s):
        return pair_out.at[:, pl.ds(pl.multiple_of(s * depth, depth), depth), :]

    def along(d, go):
        to = lax.rem(z + d, nz)
        s = slot(z, x)
        go(remote(pair_ref.at[to], pair_place(s), pz_sem.at[d], p_sem.at[s], to, x))
        go(remote(down_ref.at[to], down_out.at[s], dz_sem.at[d], d_sem.at[s], to, x))

    def across(src_pair, src_down, d, s, go):
        for e in range(1, nx):
            to = lax.rem(x + e, nx)
            go(remote(src_pair, pair_place(s), px_sem.at[e - 1, d], p_sem.at[s], z, to))
            go(remote(src_down, down_out.at[s], dx_sem.at[e - 1, d], d_sem.at[s], z, to))

    def arrived(src_pair, src_down, s):
        remote(src_pair, pair_place(s), pz_sem.at[0], p_sem.at[s], z, x).wait_recv()
        remote(src_down, down_out.at[s], dz_sem.at[0], d_sem.at[s], z, x).wait_recv()

    start = lambda copy: copy.start()
    sent = lambda copy: copy.wait_send()

    flow(kv_ref, 0, z, start)
    mine = slot(z, x)
    pair_out[:, pl.ds(pl.multiple_of(mine * depth, depth), depth), :] = pair_ref[z]
    down_out[mine] = down_ref[z]
    kv_all[mine] = kv_ref[...]
    m_ref[...] = jnp.full_like(m_ref, -jnp.inf)
    l_ref[...] = jnp.zeros_like(l_ref)
    acc_ref[...] = jnp.zeros_like(acc_ref)

    def attend(s):
        for h in range(heads):
            v = kv_all[s, :, keys + h * width : keys + (h + 1) * width]
            for m in range(2):
                lane = (2 * h + m) * HD
                k = kv_all[s, :, lane : lane + HD]
                for r in range(0, rows_all, block):
                    rows = pl.ds(r, block)
                    q = q_ref[rows, lane : lane + HD] * jnp.bfloat16(HD**-0.5)
                    attend_chunk(q, k, v, m_ref, l_ref, acc_ref, 2 * h + m, rows)

    def step(k, _):
        zz, _off = nearest(k, z, nz)
        here = kv_all.at[slot(zz, x)]

        @pl.when(k > 0)
        def _():
            remote(kv_ref, here, up_sem.at[k], kv_sem.at[slot(zz, x)], z, x).wait_recv()
            flow(here, k, zz, start)

        @pl.when(k == min(1, nz - 1))
        def _():
            for d in range(1, nz):
                along(d, start)
            across(pair_ref.at[z], down_ref.at[z], 0, mine, start)

        def column(e, _):
            other = lax.rem(x - e + nx, nx)

            @pl.when(e > 0)
            def _():
                remote(kv_ref, here, up_sem.at[k], kv_sem.at[slot(zz, other)], z, x).wait_recv()

            attend(slot(zz, other))
            return 0

        lax.fori_loop(0, nx, column, 0)
        return 0

    lax.fori_loop(0, nz, step, 0)
    for d in range(1, nz):
        zz = lax.rem(z - d + nz, nz)
        s = slot(zz, x)
        arrived(pair_ref.at[z], down_ref.at[z], s)
        across(pair_place(s), down_out.at[s], d, s, start)
    finish_heads(heads, width, lam_ref, gain_ref, l_ref, acc_ref, out_ref)
    for d in range(nz):
        zz = lax.rem(z - d + nz, nz)
        for e in range(1, nx):
            arrived(pair_ref.at[z], down_ref.at[z], slot(zz, lax.rem(x - e + nx, nx)))
    for d in range(nz):
        zz = lax.rem(z - d + nz, nz)
        s = slot(zz, x)
        across(pair_place(s), down_out.at[s], d, s, sent)
        if d:
            along(d, sent)

    def settle(k, _):
        zz, _off = nearest(k, z, nz)
        flow(kv_ref, k, zz, sent)
        return 0

    lax.fori_loop(0, nz, settle, 0)


def gather_attend(nz, nx, queries, kv, lambdas, head_gain, pairs, downs):
    rows = queries.shape[0]
    heads = lambdas.shape[0]
    width = head_gain.shape[0]
    _, _, depth, mine = pairs.shape
    blocks = nz * nx
    vmem = pl.BlockSpec(memory_space=pltpu.VMEM)
    dma = pltpu.SemaphoreType.DMA
    side = max(nx - 1, 1)
    return pl.pallas_call(
        functools.partial(gather_attend_kernel, nz, nx, heads, 256),
        out_shape=[
            jax.ShapeDtypeStruct((rows, heads * width), jnp.bfloat16),
            jax.ShapeDtypeStruct((2, blocks * depth, mine), jnp.bfloat16),
            jax.ShapeDtypeStruct((blocks,) + downs.shape[1:], jnp.bfloat16),
        ],
        in_specs=[pl.BlockSpec(memory_space=pltpu.SMEM)] + [vmem] * 5,
        out_specs=[vmem] * 3,
        scratch_shapes=[pltpu.VMEM((blocks,) + kv.shape, jnp.bfloat16)]
        + [pltpu.VMEM((2 * heads, rows, width), jnp.float32)] * 3
        + [
            dma((nz,)), dma((nz,)), dma((side, nz)), dma((blocks,)),
            dma((nz,)), dma((nz,)), dma((side, nz)), dma((side, nz)), dma((blocks,)), dma((blocks,)),
        ],
        compiler_params=pltpu.CompilerParams(
            collective_id=0, has_side_effects=True, vmem_limit_bytes=60 * 1024 * 1024
        ),
        cost_estimate=pl.CostEstimate(
            flops=rows * rows * blocks * heads * 4096, bytes_accessed=4000000, transcendentals=0
        ),
        name="gather_attend",
    )(lambdas, queries, kv, head_gain.reshape(1, width), pairs, downs)


def gather_rows_kernel(nz, nt, own_ref, out_ref, up_sem, low_sem, y_sem, c_sem, got_sem):
    z, t = lax.axis_index("z"), lax.axis_index("tp")
    rows = own_ref.shape[0]
    partner = t + 1 - 2 * lax.rem(t, 2)

    barrier = pltpu.get_barrier_semaphore()
    for a in range(nz):
        for b in range(nt):
            if a + b > 0:
                pl.semaphore_signal(
                    barrier, inc=1,
                    device_id={"z": lax.rem(z + a, nz), "tp": lax.rem(t + b, nt)},
                    device_id_type=pl.DeviceIdType.MESH,
                )
    pl.semaphore_wait(barrier, nz * nt - 1)

    def place(zz, tt):
        s = zz * nt + tt
        return out_ref.at[pl.ds(pl.multiple_of(s * rows, rows), rows), :], got_sem.at[s]

    def remote(src, zz, tt, send, to_z, to_t):
        dst, recv = place(zz, tt)
        return pltpu.make_async_remote_copy(
            src_ref=src, dst_ref=dst, send_sem=send, recv_sem=recv,
            device_id={"z": to_z, "tp": to_t}, device_id_type=pl.DeviceIdType.MESH,
        )

    def flow(src, k, zz, go):
        @pl.when(jnp.logical_and(zz <= z, z < nz - 1))
        def _():
            go(remote(src, zz, t, up_sem.at[k], jnp.minimum(z + 1, nz - 1), t))

        @pl.when(jnp.logical_and(zz >= z, z > 0))
        def _():
            go(remote(src, zz, t, low_sem.at[k], jnp.maximum(z - 1, 0), t))

        for e in range(1, nt // 2):
            go(remote(src, zz, t, y_sem.at[k, e], z, lax.rem(t + 2 * e, nt)))
        go(remote(src, zz, t, c_sem.at[k, 0], z, partner))

    start = lambda copy: copy.start()
    sent = lambda copy: copy.wait_send()

    def await_block(zz, tt):
        remote(own_ref, zz, tt, c_sem.at[0, 0], z, partner).wait_recv()

    flow(own_ref, 0, z, start)
    mine, _sem = place(z, t)
    mine[...] = own_ref[...]

    def same_core(e):
        return lax.rem(t - 2 * e + nt, nt)

    def step(k, _):
        zz, _off = nearest(k, z, nz)

        @pl.when(k > 0)
        def _():
            await_block(zz, t)
            flow(place(zz, t)[0], k, zz, start)

        for e in range(1, nt // 2):
            tt = same_core(e)
            await_block(zz, tt)
            remote(place(zz, tt)[0], zz, tt, c_sem.at[k, e], z, partner).start()
        return 0

    lax.fori_loop(0, nz, step, 0)

    def settle(k, _):
        zz, _off = nearest(k, z, nz)
        flow(own_ref, k, zz, sent)
        for e in range(nt // 2):
            await_block(zz, lax.rem(partner - 2 * e + nt, nt))
            if e:
                tt = same_core(e)
                remote(own_ref, zz, tt, c_sem.at[k, e], z, partner).wait_send()
        return 0

    lax.fori_loop(0, nz, settle, 0)


def gather_rows(nz, nt, own):
    rows, width = own.shape
    if nt % 2:
        return lax.all_gather(own, ("z", "tp"), axis=0, tiled=True)
    vmem = pl.BlockSpec(memory_space=pltpu.VMEM)
    dma = pltpu.SemaphoreType.DMA
    return pl.pallas_call(
        functools.partial(gather_rows_kernel, nz, nt),
        out_shape=jax.ShapeDtypeStruct((nz * nt * rows, width), own.dtype),
        in_specs=[vmem],
        out_specs=vmem,
        scratch_shapes=[dma((nz,)), dma((nz,)), dma((nz, nt // 2)), dma((nz, nt // 2)), dma((nz * nt,))],
        compiler_params=pltpu.CompilerParams(
            collective_id=1, has_side_effects=True, vmem_limit_bytes=32 * 1024 * 1024
        ),
        cost_estimate=pl.CostEstimate(flops=10**10, bytes_accessed=4000000, transcendentals=0),
        name="gather_rows",
    )(own)


def per_device(
    nz, nx, residual, queries, key_pairs, values, lambdas, head_gain, w_out, norm_gain, w_gate, w_up, w_down
):
    local_rows = queries.shape[0]
    heads_here = lambdas.shape[0]
    value_width = head_gain.shape[0]
    d_rows, units = w_gate.shape
    mine = units // nz
    width = residual.shape[1]

    kv = jnp.concatenate([key_pairs, values], axis=1)
    pairs = jnp.stack([w_gate.reshape(d_rows, nz, mine), w_up.reshape(d_rows, nz, mine)], axis=2)
    pairs = jnp.transpose(pairs, (1, 2, 0, 3))
    heads_out, both, downs = gather_attend(
        nz, nx, queries, kv, lambdas, head_gain, pairs, w_down.reshape(nz, mine, w_down.shape[1])
    )
    gate, up = both[0], both[1]
    down = jnp.transpose(downs, (1, 0, 2)).reshape(mine, width)
    tp_index = lax.axis_index("tp")
    own_rows = local_rows // lax.axis_size("tp")
    w_mine = lax.dynamic_slice_in_dim(
        w_out, tp_index * heads_here * value_width, heads_here * value_width, 0
    )
    projected = lax.psum_scatter(
        jnp.dot(heads_out, w_mine, preferred_element_type=jnp.float32).astype(jnp.bfloat16),
        "tp",
        scatter_dimension=0,
        tiled=True,
    ).astype(jnp.float32)
    residual_own = lax.dynamic_slice_in_dim(residual, tp_index * own_rows, own_rows, 0)
    hidden_own = (residual_own.astype(jnp.float32) + projected).astype(jnp.bfloat16)
    stream_f = hidden_own.astype(jnp.float32)
    scaled = stream_f * lax.rsqrt(jnp.mean(stream_f * stream_f, axis=-1, keepdims=True) + 1e-05)
    normed_rows = gather_rows(nz, lax.axis_size("tp"), (scaled * norm_gain).astype(jnp.bfloat16))
    gate_sum = jnp.dot(normed_rows, gate, preferred_element_type=jnp.float32)
    up_sum = jnp.dot(normed_rows, up, preferred_element_type=jnp.float32)
    hidden_units = (jax.nn.silu(gate_sum) * up_sum).astype(jnp.bfloat16)
    ffn_out = lax.psum_scatter(
        jnp.dot(hidden_units, down, preferred_element_type=jnp.float32).astype(jnp.bfloat16),
        ("z", "tp"),
        scatter_dimension=0,
        tiled=True,
    ).astype(jnp.float32)
    return (hidden_own.astype(jnp.float32) + ffn_out).astype(jnp.bfloat16)


def solution(mesh):
    sp, tp = mesh.shape["sp"], mesh.shape["tp"]
    coords = [getattr(d, "coords", None) for d in mesh.devices.flat]
    nx = len({c[0] for c in coords}) if all(c is not None for c in coords) else 2
    if sp % nx:
        nx = 1
    nz = sp // nx
    cube = Mesh(np.asarray(mesh.devices).reshape(nz, nx, tp), ("z", "x", "tp"))
    zx = ("z", "x")
    placed = (
        P(zx, None),
        P(zx, "tp"),
        P(zx, "tp"),
        P(zx, "tp"),
        P("tp"),
        P(),
        P(),
        P(),
        P(zx, "tp"),
        P(zx, "tp"),
        P("tp", zx),
    )
    return jax.shard_map(
        functools.partial(per_device, nz, nx),
        mesh=cube,
        in_specs=placed,
        out_specs=P(("z", "x", "tp"), None),
        check_vma=False,
    )
```

profile of v0, /device:TPU:20, one launch (start us, length us, event | category | flops | bytes accessed | tf_op | source)
XLA Modules:
  0.0 388.7 jit_solution(13355501681164366716)
XLA Ops:
  6.5 0.0 copy-start.1
  6.5 0.0 reduce-scatter.3.cloned.1.call-start
  6.5 0.0 copy-start.2
  6.5 0.0 copy-start.3
  6.5 1.5 copy.12
  8.0 0.4 copy.14
  8.4 0.0 copy-done.1
  8.4 0.3 copy.13
  8.7 0.4 copy.15
  9.0 0.0 copy-done.2
  9.1 0.0 copy-done.3
  9.1 0.8 pad_maximum_fusion.kv_ref
  9.9 1.4 maximum_bitcast_fusion.pair_ref
  11.3 136.3 %gather_attend.1 = (bf16[512,256]{1,0:T(8,128)(2,1)}, bf16[2,2048,352]{2,1,0:T(8,128)(2,1)}, bf16[8,352,256]{2,1,0:T(8,128)(2,1)}) custom-call(f32[2]{0:T(128)} %lam_ref.1, bf16[512,256]{1,0:T(8,128)(2,1)} %q_ref.1, bf16[512,512]{1,0:T(8,128)(2,1)} %pad_maximum_fusion.kv_ref, f32[1,128]{1,0:T(1,128)} %bitcast.25, ...), custom_call_target="tpu_custom_call" | custom-call | flops 17179869184 | bytes 4000000 | tf_op jit(solution)/shard_map/gather_attend/pallas_call | solution.py:200
  147.6 0.0 copy-start
  147.6 3.5 convolution_convert_fusion.1
  151.1 0.0 copy-start.4
  151.1 0.0 reduce-scatter.3.cloned.1.call-update
  151.2 0.2 reduce-scatter.5.cloned.1.call-start
  151.4 0.0 copy-done
  151.4 0.2 copy.17
  151.6 43.9 %reduce-scatter.3.cloned.1.call-done = bf16[128,2048]{1,0:T(8,128)(2,1)} async-done(((bf16[512,2048]{1,0:T(8,128)(2,1)}), bf16[128,2048]{1,0:T(8,128)(2,1)}) %reduce-scatter.3.cloned.1.call-update) | async-done | bytes 524304 | tf_op jit(solution)/shard_map/reduce_scatter | solution.py:350
  195.5 1.5 fusion.6
  196.9 0.0 copy-done.4
  196.9 0.2 fusion.8.own_ref
  197.1 0.0 copy-start.5
  197.1 54.0 %gather_rows.1 = bf16[2048,2048]{1,0:T(8,128)(2,1)S(1)} custom-call(bf16[128,2048]{1,0:T(8,128)(2,1)S(1)} %fusion.8.own_ref), custom_call_target="tpu_custom_call" | custom-call | flops 10000000000 | bytes 4000000 | tf_op jit(solution)/shard_map/gather_rows/pallas_call | solution.py:313
  251.1 0.0 copy-done.5
  251.2 3.3 fusion.2
  254.5 4.0 %fusion = bf16[2048,352]{0,1:T(8,128)(2,1)S(1)} fusion(bf16[2048,2048]{1,0:T(8,128)(2,1)S(1)} %gather_rows.1, f32[2048,352]{0,1:T(8,128)S(1)} %fusion.2, bf16[2,2048,352]{2,1,0:T(8,128)(2,1)S(1)} %copy-done.5), kind=kOutput, calls=%fused_computation.3 | convolution fusion | flops 2957115392 | bytes 14286848 | tf_op jit(solution)/shard_map/dot_general | solution.py:362
  258.5 6.9 %convolution_convert_fusion = bf16[2048,2048]{1,0:T(8,128)(2,1)} fusion(bf16[2048,352]{0,1:T(8,128)(2,1)S(1)} %fusion, bf16[352,2048]{1,0:T(8,128)(2,1)S(1)} %bitcast.22), kind=kOutput, calls=%fused_computation | convolution fusion | flops 2956984320 | bytes 11272192 | tf_op jit(solution)/shard_map/dot_general | solution.py:365
  265.4 0.0 reduce-scatter.5.cloned.1.call-update
  265.4 114.5 %reduce-scatter.5.cloned.1.call-done = bf16[128,2048]{1,0:T(8,128)(2,1)} async-done(((bf16[2048,2048]{1,0:T(8,128)(2,1)}), bf16[128,2048]{1,0:T(8,128)(2,1)}) %reduce-scatter.5.cloned.1.call-update) | async-done | bytes 524304 | tf_op jit(solution)/shard_map/reduce_scatter | solution.py:364
  379.9 2.0 fusion.9
  (1 shorter events, 0.0 us)
Async XLA Ops:
  6.5 1.9 copy-start.1
  6.5 188.9 %reduce-scatter.3.cloned.1.call-start = ((), (), s32[]{:S(2)}) async-start(), calls=%async_computation.2 | async-start | bytes 2621440 | tf_op jit(solution)/shard_map/reduce_scatter | solution.py:350
  6.5 2.5 copy-start.2
  6.5 2.5 copy-start.3
  147.6 3.7 copy-start
  151.1 45.8 %copy-start.4 = (f32[2048]{0:T(1024)S(1)}, f32[2048]{0:T(1024)}, u32[]{:S(2)}) copy-start(f32[2048]{0:T(1024)} %param.18) | copy-start | bytes 24580
  151.2 228.7 %reduce-scatter.5.cloned.1.call-start = ((), (), s32[]{:S(2)}) async-start(), calls=%async_computation.3 | async-start | bytes 8912896 | tf_op jit(solution)/shard_map/reduce_scatter | solution.py:364
  197.1 54.0 %copy-start.5 = (bf16[2,2048,352]{2,1,0:T(8,128)(2,1)S(1)}, bf16[2,2048,352]{2,1,0:T(8,128)(2,1)}, u32[]{:S(2)}) copy-start(bf16[2,2048,352]{2,1,0:T(8,128)(2,1)} %get-tuple-element.9) | copy-start | bytes 8650756
Sparse Core Ops, SparseCore 0:
  151.3 44.1 reduce-scatter.2
  265.5 114.3 reduce-scatter.4
where the time goes:
time: 391 us; the launch traced here: 389 us
  Pallas kernels  190 us (49%)
  waiting for transfers between devices  158 us (40%)
  matrix products  17.7 us (5%)
  between operations  13.5 us (3%)
  other arithmetic  5.9 us (2%)
    pallas_call x1, Pallas kernels, gather_attend(): pl.pallas_call(functools.partial(gather_attend_kernel, nz, nx, heads, 256...  136 us
    reduce_scatter x1, waiting for transfers between devices, per_device(): lax.psum_scatter(jnp.dot(hidden_units, down, preferred_element_type=jnp.f...  114 us
    pallas_call x1, Pallas kernels, gather_rows(): pl.pallas_call(functools.partial(gather_rows_kernel, nz, nt), out_shape=j...  54 us
    reduce_scatter x1, waiting for transfers between devices, per_device(): lax.psum_scatter(jnp.dot(heads_out, w_mine, preferred_element_type=jnp.fl...  43.9 us
  transfers between devices with their start and end apart: 2, of which 2 were waited for; matrix products, arithmetic and copies ran while one was open for 0% of the time, Pallas kernels for 0%

commit v1 on v0

--- a/solution.py
+++ b/solution.py
@@ -370,32 +370,443 @@
     return (hidden_own.astype(jnp.float32) + ffn_out).astype(jnp.bfloat16)
 
 
+def layer_kernel(
+    nz, nx, ny, nc,
+    lam_ref, q_ref, k_ref, v_ref, gain_ref, norm_ref, res_ref, wout_ref, wg_ref, wu_ref, wd_ref,
+    out_ref,
+    q_all, qm, kv, vt, m_ref, l_ref, acc, ho, hg, wout, res, hidden, xs, wgu, wd, hb, part, r1, r2, r3,
+    q_sem, kx_sem, up_sem, low_sem, kv_sem,
+    gs_sem, gr_sem, gp_sem, gq_sem, ds_sem, dr_sem, dp_sem, dq_sem,
+    hs_sem, hr_sem, in_sem, xs_sem, xr_sem, rs_sem, rr_sem,
+):
+    z, x = lax.axis_index("z"), lax.axis_index("x")
+    y, c = lax.axis_index("y"), lax.axis_index("c")
+    z0 = lax.rem(z, 2)
+    tokens = q_ref.shape[0]
+    wide = v_ref.shape[1] // nx
+    own_rows, width = out_ref.shape
+    depth = wg_ref.shape[0]
+    units, quarter = wg_ref.shape[1], wgu.shape[3]
+    tp = y * nc + c
+    xo, co = 1 - x, 1 - c
+    here = dict(z=z, x=x, y=y, c=c)
+
+    def remote(src, dst, send, recv, **to):
+        return pltpu.make_async_remote_copy(
+            src_ref=src, dst_ref=dst, send_sem=send, recv_sem=recv,
+            device_id={**here, **to}, device_id_type=pl.DeviceIdType.MESH,
+        )
+
+    def lanes(i, n):
+        return pl.ds(pl.multiple_of(i * n, n), n)
+
+    local_in = [
+        pltpu.make_async_copy(wout_ref, wout, in_sem.at[0]),
+        pltpu.make_async_copy(res_ref.at[lanes(tp, own_rows), :], res, in_sem.at[1]),
+    ]
+    for copy in local_in:
+        copy.start()
+
+    barrier = pltpu.get_barrier_semaphore()
+    peers = [dict(z=lax.rem(z + a, nz), x=lax.rem(x + b, nx)) for a in range(nz) for b in range(nx) if a + b]
+    peers += [
+        dict(x=lax.rem(x + b, nx), y=lax.rem(y + e, ny), c=lax.rem(c + f, nc))
+        for b in range(nx) for e in range(ny) for f in range(nc) if e + f
+    ]
+    for to in peers:
+        pl.semaphore_signal(barrier, inc=1, device_id={**here, **to}, device_id_type=pl.DeviceIdType.MESH)
+    pl.semaphore_wait(barrier, len(peers))
+
+    start = lambda copy: copy.start()
+    sent = lambda copy: copy.wait_send()
+
+    def slot(zz, xx):
+        return zz * nx + xx
+
+    mine = slot(z, x)
+
+    def swap(go):
+        go(remote(q_ref.at[:, lanes(xo, wide)], q_all.at[x], q_sem.at[0], q_sem.at[1], x=xo))
+        go(remote(k_ref.at[:, lanes(xo, wide)], kv.at[mine, 0], kx_sem.at[0], kv_sem.at[mine], x=xo))
+        go(remote(v_ref.at[:, lanes(xo, wide)], kv.at[mine, 1], kx_sem.at[1], kv_sem.at[mine], x=xo))
+
+    def up_down(zz, go_up, go_low):
+        @pl.when(jnp.logical_and(zz <= z, z < nz - 1))
+        def _():
+            go_up(jnp.minimum(z + 1, nz - 1))
+
+        @pl.when(jnp.logical_and(zz >= z, z > 0))
+        def _():
+            go_low(jnp.maximum(z - 1, 0))
+
+    def own_flow(sem, to):
+        for i, ref in enumerate((k_ref, v_ref)):
+            remote(ref.at[:, lanes(x, wide)], kv.at[mine, i], sem.at[mine], kv_sem.at[mine], z=to).start()
+
+    def flow(s, zz, go):
+        up_down(
+            zz,
+            lambda to: go(remote(kv.at[s], kv.at[s], up_sem.at[s], kv_sem.at[s], z=to)),
+            lambda to: go(remote(kv.at[s], kv.at[s], low_sem.at[s], kv_sem.at[s], z=to)),
+        )
+
+    def offset(q):
+        return pl.multiple_of(jnp.minimum(q * quarter, units - quarter), 128)
+
+    def target(j):
+        return lax.rem(z + j // nx, nz), lax.rem(x + lax.rem(j, nx), nx)
+
+    def gate_up(j, go):
+        zd, xd = target(j)
+        cols = pl.ds(offset(xd * 2 + lax.rem(zd, 2)), quarter)
+        rows = lanes(mine, depth)
+        for i, ref in enumerate((wg_ref, wu_ref)):
+            go(remote(ref.at[:, cols], wgu.at[c, i, rows, :], gs_sem.at[j, i], gr_sem.at[mine], z=zd, x=xd))
+
+    def downward(j, go):
+        zd, xd = target(j)
+        rows = pl.ds(offset(xd * 2 + lax.rem(zd, 2)), quarter)
+        go(remote(wd_ref.at[rows, :], wd.at[c, :, lanes(mine, depth)], ds_sem.at[j], dr_sem.at[mine], z=zd, x=xd))
+
+    q_me = x * 2 + z0
+    own_weights = [
+        pltpu.make_async_copy(ref.at[:, pl.ds(offset(q_me), quarter)], wgu.at[c, i, lanes(mine, depth), :], in_sem.at[2 + i])
+        for i, ref in enumerate((wg_ref, wu_ref))
+    ]
+    own_weights.append(
+        pltpu.make_async_copy(wd_ref.at[pl.ds(offset(q_me), quarter), :], wd.at[c, :, lanes(mine, depth)], in_sem.at[4])
+    )
+
+    swap(start)
+    up_down(z, lambda to: own_flow(up_sem, to), lambda to: own_flow(low_sem, to))
+    for copy in own_weights:
+        copy.start()
+
+    kv[mine, 0] = k_ref[:, lanes(x, wide)]
+    kv[mine, 1] = v_ref[:, lanes(x, wide)]
+    q_all[x] = q_ref[:, lanes(x, wide)]
+    m_ref[...] = jnp.full_like(m_ref, -jnp.inf)
+    l_ref[...] = jnp.zeros_like(l_ref)
+    acc[...] = jnp.zeros_like(acc)
+
+    remote(q_all.at[x], q_all.at[xo], q_sem.at[0], q_sem.at[1], x=xo).wait_recv()
+    first_map = lax.broadcasted_iota(jnp.int32, (tokens, 2 * HD), 1) < HD
+    for h in range(nx):
+        q = q_all[h].astype(jnp.float32) * HD**-0.5
+        qm[2 * h] = jnp.where(first_map, q, 0.0).astype(jnp.bfloat16)
+        qm[2 * h + 1] = jnp.where(first_map, 0.0, q).astype(jnp.bfloat16)
+
+    def attend(s):
+        vt[...] = kv[s, 1].astype(jnp.float32).T.astype(jnp.bfloat16)
+
+        def one(i, _):
+            scores = lax.dot_general(
+                kv[s, 0], qm[i], (((1,), (1,)), ((), ())), preferred_element_type=jnp.float32
+            )
+            old = m_ref[i]
+            high = jnp.maximum(old, jnp.max(scores, axis=0, keepdims=True))
+            shrink = jnp.exp(old - high)
+            weights = jnp.exp(scores - high)
+            l_ref[i] = l_ref[i] * shrink + jnp.sum(weights, axis=0, keepdims=True)
+            m_ref[i] = high
+            acc[i] = acc[i] * shrink + jnp.dot(
+                vt[...], weights.astype(jnp.bfloat16), preferred_element_type=jnp.float32
+            )
+            return 0
+
+        lax.fori_loop(0, 2 * nx, one, 0)
+
+    def step(j, _):
+        zz, _off = nearest(j // nx, z, nz)
+        xx = lax.rem(x + lax.rem(j, nx), nx)
+        s = slot(zz, xx)
+
+        @pl.when(j > 0)
+        def _():
+            remote(kv.at[s], kv.at[s], kx_sem.at[0], kv_sem.at[s], x=xo).wait_recv()
+            flow(s, zz, start)
+
+        for k, at in enumerate(GATE_STEPS, 1):
+            @pl.when(j == at)
+            def _():
+                gate_up(k, start)
+
+        attend(s)
+        return 0
+
+    lax.fori_loop(0, nz * nx, step, 0)
+
+    for h in range(nx):
+        first = acc[2 * h] / l_ref[2 * h]
+        second = acc[2 * h + 1] / l_ref[2 * h + 1]
+        differ = first - lam_ref[x] * second
+        scale = lax.rsqrt(jnp.mean(differ * differ, axis=0, keepdims=True) + 1e-05)
+        ho[h] = (differ * scale * gain_ref[...]).T.astype(jnp.bfloat16)
+
+    head = tp * nx + x
+    me = (x * ny + y) * nc + c
+
+    def spread(go):
+        n = 0
+        for b in range(nx):
+            for e in range(ny):
+                for f in range(nc):
+                    if b + e + f:
+                        xd, yd, cd = lax.rem(x + b, nx), lax.rem(y + e, ny), lax.rem(c + f, nc)
+                        src = ho.at[xd, lanes(yd * nc + cd, own_rows), :]
+                        go(remote(src, hg.at[:, lanes(head, wide)], hs_sem.at[n], hr_sem.at[me], x=xd, y=yd, c=cd))
+                        n += 1
+
+    spread(start)
+    hg[:, lanes(head, wide)] = ho[x, lanes(tp, own_rows), :]
+    for copy in local_in:
+        copy.wait()
+    for b in range(nx):
+        for e in range(ny):
+            for f in range(nc):
+                if b + e + f:
+                    xd, yd, cd = lax.rem(x + b, nx), lax.rem(y + e, ny), lax.rem(c + f, nc)
+                    other = (xd * ny + yd) * nc + cd
+                    block = hg.at[:, lanes((yd * nc + cd) * nx + xd, wide)]
+                    remote(block, block, hs_sem.at[0], hr_sem.at[other], x=xo).wait_recv()
+
+    state = res[...].astype(jnp.float32) + jnp.dot(hg[...], wout[...], preferred_element_type=jnp.float32)
+    hidden[...] = state.astype(jnp.bfloat16)
+    stream = hidden[...].astype(jnp.float32)
+    scaled = stream * lax.rsqrt(jnp.mean(stream * stream, axis=1, keepdims=True) + 1e-05)
+    cube = z0 * 4 + x * 2 + y
+    xs[cube] = (scaled * norm_ref[...]).astype(jnp.bfloat16)
+
+    bits = dict(z=(z0, 4), x=(x, 2), y=(y, 1))
+    across = dict(z=dict(z=z + 1 - 2 * z0), x=dict(x=xo), y=dict(y=1 - y))
+    orders = (("x", "y", "z"), ("y", "z", "x"), ("z", "x", "y"))
+    tiles = width // 128
+    cuts = [0] + [128 * ((tiles * (i + 1) + 2) // 3) for i in range(3)]
+    columns = [pl.ds(cuts[i], cuts[i + 1] - cuts[i]) for i in range(3)]
+
+    def flip(axis):
+        bit, mask = bits[axis]
+        return (1 - 2 * bit) * mask
+
+    def gather(p, k, go):
+        held = [cube]
+        for axis in orders[p][:k]:
+            held += [i + flip(axis) for i in held]
+        axis = orders[p][k]
+        for n, i in enumerate(held):
+            block = xs.at[i, :, columns[p]]
+            go(remote(block, block, xs_sem.at[p, k, n], xr_sem.at[p, k], **across[axis]))
+
+    def gathered(p, k):
+        block = xs.at[pl.ds(0, 2**k), :, columns[p]]
+        remote(block, block, xs_sem.at[p, k, 0], xr_sem.at[p, k], x=xo).wait_recv()
+
+    for k in range(3):
+        for p in range(3):
+            if k:
+                gathered(p, k - 1)
+            gather(p, k, start)
+
+    for j in range(1, nz * nx):
+        downward(j, start)
+    for copy in own_weights:
+        copy.wait()
+
+    def fill(weights, recv, pass_s, pass_r, take):
+        def one(j, _):
+            s = lax.rem(mine + j, nz * nx)
+
+            @pl.when(j > 0)
+            def _():
+                remote(take(c, s), take(c, s), pass_s.at[s], recv.at[s], c=co).wait_recv()
+
+            remote(take(c, s), take(c, s), pass_s.at[s], pass_r.at[s], c=co).start()
+            return 0
+
+        lax.fori_loop(0, nz * nx, one, 0)
+
+        def end(s, _):
+            remote(take(co, s), take(co, s), pass_s.at[s], pass_r.at[s], c=co).wait_recv()
+            return 0
+
+        lax.fori_loop(0, nz * nx, end, 0)
+
+    fill(wgu, gr_sem, gp_sem, gq_sem, lambda cc, s: wgu.at[cc, :, lanes(s, depth), :])
+    for p in range(3):
+        gathered(p, 2)
+
+    rows = 2 * own_rows
+    blocks = 8
+    spare = q_me * quarter - jnp.minimum(q_me * quarter, units - quarter)
+    keep = lax.broadcasted_iota(jnp.int32, (rows, quarter), 1) >= spare
+
+    def expand(i, _):
+        both = xs[pl.ds(2 * i, 2)].reshape(rows, width)
+        for cc in range(nc):
+            gate = jnp.dot(both, wgu[cc, 0], preferred_element_type=jnp.float32)
+            up = jnp.dot(both, wgu[cc, 1], preferred_element_type=jnp.float32)
+            made = gate / (1.0 + jnp.exp(-gate)) * up
+            hb[lanes(i, rows), cc * quarter : (cc + 1) * quarter] = jnp.where(keep, made, 0.0).astype(jnp.bfloat16)
+        return 0
+
+    lax.fori_loop(0, blocks // 2, expand, 0)
+    fill(wd, dr_sem, dp_sem, dq_sem, lambda cc, s: wd.at[cc, :, lanes(s, depth)])
+
+    def place(p, flips):
+        return cube + sum(flip(axis) for axis in flips)
+
+    def choices(axes):
+        sets = [()]
+        for axis in axes:
+            sets = sets + [t + (axis,) for t in sets]
+        return sets
+
+    held_in = (r1, r2, r3)
+
+    def reduce_send(p, k, go):
+        axis, rest = orders[p][k], orders[p][k + 1 :]
+        for n, t in enumerate(choices(rest)):
+            spot = sum((bits[a][0] if a not in t else 1 - bits[a][0]) * 2**i for i, a in enumerate(rest))
+            src = part.at[place(p, t + (axis,)), :, columns[p]]
+            dst = held_in[k].at[spot, :, columns[p]]
+            go(remote(src, dst, rs_sem.at[p, k, n], rr_sem.at[p, k], **across[axis]))
+
+    def reduce_take(p, k):
+        axis, rest = orders[p][k], orders[p][k + 1 :]
+        block = held_in[k].at[:, :, columns[p]]
+        remote(block, block, rs_sem.at[p, k, 0], rr_sem.at[p, k], x=xo).wait_recv()
+        if not rest:
+            return
+        for t in reversed(choices(rest)):
+            spot = sum((bits[a][0] if a not in t else 1 - bits[a][0]) * 2**i for i, a in enumerate(rest))
+            i = place(p, t)
+            part[i, :, columns[p]] = (
+                part[i, :, columns[p]].astype(jnp.float32)
+                + held_in[k][spot, :, columns[p]].astype(jnp.float32)
+            ).astype(jnp.bfloat16)
+
+    for p in range(3):
+        def contract(i, _):
+            weights = wd[:, :, columns[p]].reshape(nc * quarter, columns[p].size)
+            made = jnp.dot(hb[lanes(i, rows), :], weights, preferred_element_type=jnp.float32)
+            part[pl.ds(2 * i, 2), :, columns[p]] = made.astype(jnp.bfloat16).reshape(2, own_rows, columns[p].size)
+            return 0
+
+        lax.fori_loop(0, blocks // 2, contract, 0)
+        reduce_send(p, 0, start)
+    for k in range(2):
+        for p in range(3):
+            reduce_take(p, k)
+            reduce_send(p, k + 1, start)
+    for p in range(3):
+        reduce_take(p, 2)
+        cols = columns[p]
+        out_ref[:, cols] = (
+            hidden[:, cols].astype(jnp.float32)
+            + part[cube, :, cols].astype(jnp.float32)
+            + r3[0, :, cols].astype(jnp.float32)
+        ).astype(jnp.bfloat16)
+
+    swap(sent)
+
+    def settle(j, _):
+        zz, _off = nearest(j // nx, z, nz)
+        flow(slot(zz, lax.rem(x + lax.rem(j, nx), nx)), zz, sent)
+        return 0
+
+    lax.fori_loop(0, nz * nx, settle, 0)
+    for j in range(1, nz * nx):
+        gate_up(j, sent)
+        downward(j, sent)
+    spread(sent)
+    for p in range(3):
+        for k in range(3):
+            gather(p, k, sent)
+            reduce_send(p, k, sent)
+
+    def passed(s, _):
+        block = wgu.at[c, :, lanes(s, depth), :]
+        remote(block, block, gp_sem.at[s], gq_sem.at[s], c=co).wait_send()
+        block = wd.at[c, :, lanes(s, depth)]
+        remote(block, block, dp_sem.at[s], dq_sem.at[s], c=co).wait_send()
+        return 0
+
+    lax.fori_loop(0, nz * nx, passed, 0)
+
+
+GATE_STEPS = (2, 3, 4, 5, 6, 7, 7)
+
+
+def layer(
+    nz, nx, ny, nc, residual, queries, key_pairs, values, lambdas, head_gain, w_out, norm_gain, w_gate, w_up, w_down
+):
+    tokens = queries.shape[0]
+    wide = head_gain.shape[0]
+    width = residual.shape[1]
+    depth, units = w_gate.shape
+    own_rows = tokens // (ny * nc)
+    quarter = -(-units // (2 * nx * 128)) * 128
+    vmem = pl.BlockSpec(memory_space=pltpu.VMEM)
+    hbm = pl.BlockSpec(memory_space=pl.ANY)
+    dma = pltpu.SemaphoreType.DMA
+    bf16 = lambda *shape: pltpu.VMEM(shape, jnp.bfloat16)
+    f32 = lambda *shape: pltpu.VMEM(shape, jnp.float32)
+    n = nz * nx
+    return pl.pallas_call(
+        functools.partial(layer_kernel, nz, nx, ny, nc),
+        out_shape=jax.ShapeDtypeStruct((own_rows, width), jnp.bfloat16),
+        in_specs=[pl.BlockSpec(memory_space=pltpu.SMEM)] + [vmem] * 5 + [hbm] * 5,
+        out_specs=vmem,
+        scratch_shapes=[
+            bf16(nx, tokens, wide), bf16(2 * nx, tokens, wide), bf16(n, 2, tokens, wide), bf16(wide, tokens),
+            f32(2 * nx, 1, tokens), f32(2 * nx, 1, tokens), f32(2 * nx, wide, tokens),
+            bf16(nx, tokens, wide), bf16(own_rows, w_out.shape[0]),
+            bf16(*w_out.shape), bf16(own_rows, width), bf16(own_rows, width),
+            bf16(8, own_rows, width), bf16(nc, 2, width, quarter), bf16(nc, quarter, width),
+            bf16(8 * own_rows, nc * quarter), bf16(8, own_rows, width),
+            bf16(4, own_rows, width), bf16(2, own_rows, width), bf16(1, own_rows, width),
+            dma((2,)), dma((2,)), dma((n,)), dma((n,)), dma((n,)),
+            dma((n, 2)), dma((n,)), dma((n,)), dma((n,)), dma((n,)), dma((n,)), dma((n,)), dma((n,)),
+            dma((nx * ny * nc,)), dma((nx * ny * nc,)), dma((5,)),
+            dma((3, 3, 4)), dma((3, 3)), dma((3, 3, 4)), dma((3, 3)),
+        ],
+        compiler_params=pltpu.CompilerParams(
+            collective_id=2, has_side_effects=True, vmem_limit_bytes=62 * 1024 * 1024
+        ),
+        name="layer",
+    )(
+        lambdas, queries, key_pairs, values, head_gain.reshape(wide, 1), norm_gain.reshape(1, width),
+        residual, w_out, w_gate, w_up, w_down,
+    )
+
+
 def solution(mesh):
     sp, tp = mesh.shape["sp"], mesh.shape["tp"]
     coords = [getattr(d, "coords", None) for d in mesh.devices.flat]
-    nx = len({c[0] for c in coords}) if all(c is not None for c in coords) else 2
+    known = all(p is not None for p in coords)
+    nx = len({p[0] for p in coords}) if known else 2
+    ny = len({p[1] for p in coords}) if known else 2
     if sp % nx:
         nx = 1
-    nz = sp // nx
-    cube = Mesh(np.asarray(mesh.devices).reshape(nz, nx, tp), ("z", "x", "tp"))
-    zx = ("z", "x")
-    placed = (
-        P(zx, None),
-        P(zx, "tp"),
-        P(zx, "tp"),
-        P(zx, "tp"),
-        P("tp"),
-        P(),
-        P(),
-        P(),
-        P(zx, "tp"),
-        P(zx, "tp"),
-        P("tp", zx),
-    )
-    return jax.shard_map(
-        functools.partial(per_device, nz, nx),
-        mesh=cube,
-        in_specs=placed,
-        out_specs=P(("z", "x", "tp"), None),
-        check_vma=False,
-    )
+    if tp % ny:
+        ny = 1
+    nz, nc = sp // nx, tp // ny
+    zx, yc = ("z", "x"), ("y", "c")
+
+    def placed(tp_axes):
+        split = P(zx, tp_axes)
+        return (P(zx, None), split, split, split, P(tp_axes), P(), P(), P(), split, split, P(tp_axes, zx))
+
+    def run(*args):
+        heads, units = args[4].shape[0], args[8].shape[1] // tp
+        if nx == ny == nc == 2 and nz % 2 == 0 and heads == tp * nx and units % 128 == 0:
+            box = Mesh(np.asarray(mesh.devices).reshape(nz, nx, ny, nc), ("z", "x", "y", "c"))
+            body, tp_axes = functools.partial(layer, nz, nx, ny, nc), yc
+        else:
+            box = Mesh(np.asarray(mesh.devices).reshape(nz, nx, tp), ("z", "x", "tp"))
+            body, tp_axes = functools.partial(per_device, nz, nx), ("tp",)
+        return jax.shard_map(
+            body, mesh=box, in_specs=placed(tp_axes), out_specs=P(zx + tp_axes, None), check_vma=False
+        )(*args)
+
+    return run

time: 391 us -> 219 us (0.56)
  waiting for transfers between devices: 158 us -> 0 us
  Pallas kernels: 190 us -> 215 us
  matrix products: 17.7 us -> 0 us
  between operations: 13.5 us -> 0.01 us
  other arithmetic: 5.9 us -> 0 us
    reduce_scatter x2 -> x0, waiting for transfers between devices: 158 us -> none  [the longest x1 114 us: per_device(): lax.psum_scatter(jnp.dot(hidden_units, down, preferred_element_type=jnp.f...]
    pallas_call x2 -> x1, Pallas kernels: 190 us -> 215 us  [layer(): pl.pallas_call(functools.partial(layer_kernel, nz, nx, ny, nc), out_shape...]
    dot_general x4 -> x0, matrix products: 17.7 us -> none  [the longest x1 6.91 us: per_device(): jnp.dot(hidden_units, down, preferred_element_type=jnp.float32)]
  transfers between devices with their start and end apart: 2 -> 0, of which waited for: 2 -> 0; matrix products, arithmetic and copies ran while one was open for 0% -> 0% of each run, Pallas kernels for 0% -> 0%
where the time goes in v1:
time: 219 us; the launch traced here: 218 us
  Pallas kernels  215 us (98%)
  local copies, waits for them, and re-layouts  3.27 us (1%)
    pallas_call x1, Pallas kernels, layer(): pl.pallas_call(functools.partial(layer_kernel, nz, nx, ny, nc), out_shape...  215 us

profile of v1, /device:TPU:20, one launch (start us, length us, event | category | flops | bytes accessed | tf_op | source)
XLA Modules:
  0.0 218.4 jit_solution(10561812721415786470)
XLA Ops:
  0.0 1.4 copy.12.gain_ref
  1.4 215.1 %layer.1 = bf16[128,2048]{1,0:T(8,128)(2,1)} custom-call(f32[2]{0:T(128)} %lam_ref.1, bf16[512,256]{1,0:T(8,128)(2,1)} %q_ref.1, bf16[512,256]{1,0:T(8,128)(2,1)} %k_ref.1, bf16[512,256]{1,0:T(8,128)(2,1)} %v_ref.1, f32[128,1]{1,0:T(8,128)} %copy.12.gain_ref, f32[1,2048]{1,0:T(1,128)} %bitcast.2, bf16[512,2048]{1,0:T(8,128)(2,1)} %res_ref.1, ...), custom_call_target="tpu_custom_call" | custom-call | tf_op jit(solution)/shard_map/layer/pallas_call | solution.py:755
  216.5 1.9 copy.14

commit v2 on v1

--- a/solution.py
+++ b/solution.py
@@ -374,10 +374,10 @@
     nz, nx, ny, nc,
     lam_ref, q_ref, k_ref, v_ref, gain_ref, norm_ref, res_ref, wout_ref, wg_ref, wu_ref, wd_ref,
     out_ref,
-    q_all, qm, kv, vt, m_ref, l_ref, acc, ho, hg, wout, res, hidden, xs, wgu, wd, hb, part, r1, r2, r3,
+    q_all, qm, kv, vt, m_ref, l_ref, acc, ho, hg, wout, res, hidden, xs, wgu, wd, stage, stage_d, hb, part, r1, r2, r3,
     q_sem, kx_sem, up_sem, low_sem, kv_sem,
     gs_sem, gr_sem, gp_sem, gq_sem, ds_sem, dr_sem, dp_sem, dq_sem,
-    hs_sem, hr_sem, in_sem, xs_sem, xr_sem, rs_sem, rr_sem,
+    wx_sem, st_sem, hs_sem, hr_sem, in_sem, xz_sem, xs_sem, xr_sem, rs_sem, rr_sem,
 ):
     z, x = lax.axis_index("z"), lax.axis_index("x")
     y, c = lax.axis_index("y"), lax.axis_index("c")
@@ -453,21 +453,53 @@
     def offset(q):
         return pl.multiple_of(jnp.minimum(q * quarter, units - quarter), 128)
 
-    def target(j):
-        return lax.rem(z + j // nx, nz), lax.rem(x + lax.rem(j, nx), nx)
-
-    def gate_up(j, go):
-        zd, xd = target(j)
-        cols = pl.ds(offset(xd * 2 + lax.rem(zd, 2)), quarter)
+    halves = nz // 2
+
+    def half(g):
+        return lax.rem(z // 2 + g, halves)
+
+    near = [(0, 1, b) for b in range(nx)]
+    far = [(g, t, b) for b in range(nx) for g in range(1, halves) for t in range(2)]
+
+    def units_of(xd, t):
+        return pl.ds(offset(xd * 2 + lax.rem(z0 + t, 2)), quarter)
+
+    def aside(go):
         rows = lanes(mine, depth)
         for i, ref in enumerate((wg_ref, wu_ref)):
-            go(remote(ref.at[:, cols], wgu.at[c, i, rows, :], gs_sem.at[j, i], gr_sem.at[mine], z=zd, x=xd))
-
-    def downward(j, go):
-        zd, xd = target(j)
-        rows = pl.ds(offset(xd * 2 + lax.rem(zd, 2)), quarter)
-        go(remote(wd_ref.at[rows, :], wd.at[c, :, lanes(mine, depth)], ds_sem.at[j], dr_sem.at[mine], z=zd, x=xd))
-
+            go(remote(ref.at[:, units_of(xo, 0)], wgu.at[c, i, rows, :], wx_sem.at[0, i], gr_sem.at[mine], x=xo))
+        for i, ref in enumerate((wg_ref, wu_ref)):
+            go(remote(ref.at[:, units_of(xo, 1)], stage.at[i], wx_sem.at[1, i], st_sem.at[0], x=xo))
+        go(remote(wd_ref.at[units_of(xo, 0), :], wd.at[c, :, rows], wx_sem.at[0, 2], dr_sem.at[mine], x=xo))
+        go(remote(wd_ref.at[units_of(xo, 1), :], stage_d, wx_sem.at[1, 2], st_sem.at[1], x=xo))
+
+    def gate_up(to, go):
+        g, t, b = to
+        s = slot(z, lax.rem(x + b, nx))
+        rows = lanes(s, depth)
+        for i, ref in enumerate((wg_ref, wu_ref)):
+            src = stage.at[i] if b and t else wgu.at[c, i, rows, :] if b else ref.at[:, units_of(x, t)]
+            zd = half(g) * 2 + lax.rem(z0 + t, 2)
+            go(remote(src, wgu.at[c, i, rows, :], gs_sem.at[g, t, b, i], gr_sem.at[s], z=zd))
+
+    def downward(to, go):
+        g, t, b = to
+        s = slot(z, lax.rem(x + b, nx))
+        cols = lanes(s, depth)
+        src = stage_d if b and t else wd.at[c, :, cols] if b else wd_ref.at[units_of(x, t), :]
+        zd = half(g) * 2 + lax.rem(z0 + t, 2)
+        go(remote(src, wd.at[c, :, cols], ds_sem.at[g, t, b], dr_sem.at[s], z=zd))
+
+    def aside_came():
+        rows = lanes(slot(z, xo), depth)
+        for block, sem in (
+            (wgu.at[c, :, rows, :], gr_sem.at[slot(z, xo)]), (stage, st_sem.at[0]),
+            (wd.at[c, :, rows], dr_sem.at[slot(z, xo)]), (stage_d, st_sem.at[1]),
+        ):
+            remote(block, block, wx_sem.at[0, 0], sem, x=xo).wait_recv()
+
+    inner = z0 == jnp.where(z < nz // 2, 1, 0)
+    outer = jnp.logical_not(inner)
     q_me = x * 2 + z0
     own_weights = [
         pltpu.make_async_copy(ref.at[:, pl.ds(offset(q_me), quarter)], wgu.at[c, i, lanes(mine, depth), :], in_sem.at[2 + i])
@@ -479,6 +511,7 @@
 
     swap(start)
     up_down(z, lambda to: own_flow(up_sem, to), lambda to: own_flow(low_sem, to))
+    aside(start)
     for copy in own_weights:
         copy.start()
 
@@ -516,21 +549,37 @@
 
         lax.fori_loop(0, 2 * nx, one, 0)
 
+    def turn(j):
+        mixed = jnp.logical_and(j >= nx, j < 3 * nx) if nz > 2 else False
+        k = jnp.where(mixed, 1 + lax.rem(j, 2), j // nx)
+        e = jnp.where(mixed, (j - nx) // 2, lax.rem(j, nx))
+        zz, _off = nearest(k, z, nz)
+        return zz, slot(zz, lax.rem(x + e, nx))
+
     def step(j, _):
-        zz, _off = nearest(j // nx, z, nz)
-        xx = lax.rem(x + lax.rem(j, nx), nx)
-        s = slot(zz, xx)
+        zz, s = turn(j)
 
         @pl.when(j > 0)
         def _():
             remote(kv.at[s], kv.at[s], kx_sem.at[0], kv_sem.at[s], x=xo).wait_recv()
             flow(s, zz, start)
 
-        for k, at in enumerate(GATE_STEPS, 1):
-            @pl.when(j == at)
+        def issue(at, where, some):
+            @pl.when(jnp.logical_and(where, j == min(at, nz * nx - 1)))
             def _():
-                gate_up(k, start)
-
+                for to in some:
+                    gate_up(to, start)
+
+        issue(2, outer, [to for to in far if to[1:] == (0, 0)])
+
+        @pl.when(j == min(5, nz * nx - 1))
+        def _():
+            aside_came()
+
+        issue(5, outer, [to for to in far if to[1:] == (0, 1)])
+        issue(5, inner, [to for to in far if to[1:] == (1, 0)])
+        issue(5, outer, [to for to in far if to[1] == 1])
+        issue(7, inner, [to for to in far if to[1:] == (1, 1)])
         attend(s)
         return 0
 
@@ -579,69 +628,94 @@
 
     bits = dict(z=(z0, 4), x=(x, 2), y=(y, 1))
     across = dict(z=dict(z=z + 1 - 2 * z0), x=dict(x=xo), y=dict(y=1 - y))
-    orders = (("x", "y", "z"), ("y", "z", "x"), ("z", "x", "y"))
-    tiles = width // 128
-    cuts = [0] + [128 * ((tiles * (i + 1) + 2) // 3) for i in range(3)]
-    columns = [pl.ds(cuts[i], cuts[i + 1] - cuts[i]) for i in range(3)]
+    paths = (("x", "y"), ("y", "x"))
+    split = width // 256 * 128
+    columns = (pl.ds(0, split), pl.ds(split, width - split))
 
     def flip(axis):
         bit, mask = bits[axis]
         return (1 - 2 * bit) * mask
 
-    def gather(p, k, go):
-        held = [cube]
-        for axis in orders[p][:k]:
-            held += [i + flip(axis) for i in held]
-        axis = orders[p][k]
+    over = cube + flip("z")
+
+    def lend(go):
+        go(remote(xs.at[cube], xs.at[cube], xz_sem.at[0], xz_sem.at[1], **across["z"]))
+
+    def gather(h, p, k, go):
+        held = [(cube, over)[h]]
+        if k:
+            held += [held[0] + flip(paths[p][0])]
         for n, i in enumerate(held):
             block = xs.at[i, :, columns[p]]
-            go(remote(block, block, xs_sem.at[p, k, n], xr_sem.at[p, k], **across[axis]))
-
-    def gathered(p, k):
+            go(remote(block, block, xs_sem.at[h, p, k, n], xr_sem.at[h, p, k], **across[paths[p][k]]))
+
+    def gathered(h, p, k):
         block = xs.at[pl.ds(0, 2**k), :, columns[p]]
-        remote(block, block, xs_sem.at[p, k, 0], xr_sem.at[p, k], x=xo).wait_recv()
-
-    for k in range(3):
-        for p in range(3):
-            if k:
-                gathered(p, k - 1)
-            gather(p, k, start)
-
-    for j in range(1, nz * nx):
-        downward(j, start)
+        remote(block, block, xs_sem.at[h, p, k, 0], xr_sem.at[h, p, k], x=xo).wait_recv()
+
+    lend(start)
+    for p in range(2):
+        gather(0, p, 0, start)
+    for to in near:
+        gate_up(to, start)
+    for p in range(2):
+        gathered(0, p, 0)
+        gather(0, p, 1, start)
+
+    @pl.when(inner)
+    def _():
+        for to in far:
+            if to[1] == 0:
+                gate_up(to, start)
+
+    remote(xs.at[over], xs.at[over], xz_sem.at[0], xz_sem.at[1], x=xo).wait_recv()
+    for p in range(2):
+        gather(1, p, 0, start)
+    for p in range(2):
+        gathered(1, p, 0)
+        gather(1, p, 1, start)
+
+    @pl.when(outer)
+    def _():
+        for to in near:
+            downward(to, start)
+
     for copy in own_weights:
         copy.wait()
 
-    def fill(weights, recv, pass_s, pass_r, take):
-        def one(j, _):
-            s = lax.rem(mine + j, nz * nx)
-
-            @pl.when(j > 0)
-            def _():
-                remote(take(c, s), take(c, s), pass_s.at[s], recv.at[s], c=co).wait_recv()
-
-            remote(take(c, s), take(c, s), pass_s.at[s], pass_r.at[s], c=co).start()
-            return 0
-
-        lax.fori_loop(0, nz * nx, one, 0)
-
-        def end(s, _):
-            remote(take(co, s), take(co, s), pass_s.at[s], pass_r.at[s], c=co).wait_recv()
-            return 0
-
-        lax.fori_loop(0, nz * nx, end, 0)
-
-    fill(wgu, gr_sem, gp_sem, gq_sem, lambda cc, s: wgu.at[cc, :, lanes(s, depth), :])
-    for p in range(3):
-        gathered(p, 2)
-
-    rows = 2 * own_rows
-    blocks = 8
+    def pass_on(s, go):
+        block = wgu.at[c, :, lanes(s, depth), :]
+        go(remote(block, block, gp_sem.at[s], gq_sem.at[s], c=co))
+
+    def fill(j, _):
+        s = lax.rem(half(0) * 2 * nx + j, nz * nx)
+
+        @pl.when(s // nx != z)
+        def _():
+            block = wgu.at[c, :, lanes(s, depth), :]
+            remote(block, block, gp_sem.at[s], gr_sem.at[s], c=co).wait_recv()
+
+        pass_on(s, start)
+        return 0
+
+    def filled(s, _):
+        block = wgu.at[co, :, lanes(s, depth), :]
+        remote(block, block, gp_sem.at[s], gq_sem.at[s], c=co).wait_recv()
+        return 0
+
+    lax.fori_loop(0, nz * nx, fill, 0)
+    lax.fori_loop(0, nz * nx, filled, 0)
+    for h in range(2):
+        for p in range(2):
+            gathered(h, p, 1)
+
+    blocks, group = 8, 4
+    rows = group * own_rows
     spare = q_me * quarter - jnp.minimum(q_me * quarter, units - quarter)
     keep = lax.broadcasted_iota(jnp.int32, (rows, quarter), 1) >= spare
 
     def expand(i, _):
-        both = xs[pl.ds(2 * i, 2)].reshape(rows, width)
+        both = xs[pl.ds(group * i, group)].reshape(rows, width)
         for cc in range(nc):
             gate = jnp.dot(both, wgu[cc, 0], preferred_element_type=jnp.float32)
             up = jnp.dot(both, wgu[cc, 1], preferred_element_type=jnp.float32)
@@ -649,9 +723,14 @@
             hb[lanes(i, rows), cc * quarter : (cc + 1) * quarter] = jnp.where(keep, made, 0.0).astype(jnp.bfloat16)
         return 0
 
-    lax.fori_loop(0, blocks // 2, expand, 0)
-    fill(wd, dr_sem, dp_sem, dq_sem, lambda cc, s: wd.at[cc, :, lanes(s, depth)])
-
+    @pl.when(inner)
+    def _():
+        for to in near:
+            downward(to, start)
+
+    for to in far:
+        downward(to, start)
+    lax.fori_loop(0, blocks // group, expand, 0)
     def place(p, flips):
         return cube + sum(flip(axis) for axis in flips)
 
@@ -662,79 +741,112 @@
         return sets
 
     held_in = (r1, r2, r3)
-
-    def reduce_send(p, k, go):
+    orders = (("x", "y", "z"), ("y", "z", "x"), ("z", "x", "y"))
+    span = width // halves
+    tiles = span // 128
+    cuts = [0] + [128 * ((tiles * (i + 1) + 2) // 3) for i in range(3)]
+
+    def share(g, p):
+        return pl.ds(pl.multiple_of(half(g) * span + cuts[p], 128), cuts[p + 1] - cuts[p])
+
+    def down_on(g, go):
+        block = wd.at[c, :, lanes(half(g), span)]
+        go(remote(block, block, dp_sem.at[g], dq_sem.at[g], c=co))
+
+    def down_fill(g):
+        for n in range(2 * nx):
+            s = half(g) * 2 * nx + n
+
+            @pl.when(s // nx != z)
+            def _():
+                block = wd.at[c, :, lanes(s, depth)]
+                remote(block, block, dp_sem.at[g], dr_sem.at[s], c=co).wait_recv()
+
+        down_on(g, start)
+        block = wd.at[co, :, lanes(half(g), span)]
+        remote(block, block, dp_sem.at[g], dq_sem.at[g], c=co).wait_recv()
+
+    def reduce_send(g, p, k, go):
         axis, rest = orders[p][k], orders[p][k + 1 :]
         for n, t in enumerate(choices(rest)):
             spot = sum((bits[a][0] if a not in t else 1 - bits[a][0]) * 2**i for i, a in enumerate(rest))
-            src = part.at[place(p, t + (axis,)), :, columns[p]]
-            dst = held_in[k].at[spot, :, columns[p]]
-            go(remote(src, dst, rs_sem.at[p, k, n], rr_sem.at[p, k], **across[axis]))
-
-    def reduce_take(p, k):
+            src = part.at[place(p, t + (axis,)), :, share(g, p)]
+            dst = held_in[k].at[spot, :, share(g, p)]
+            go(remote(src, dst, rs_sem.at[g, p, k, n], rr_sem.at[g, p, k], **across[axis]))
+
+    def reduce_take(g, p, k):
         axis, rest = orders[p][k], orders[p][k + 1 :]
-        block = held_in[k].at[:, :, columns[p]]
-        remote(block, block, rs_sem.at[p, k, 0], rr_sem.at[p, k], x=xo).wait_recv()
-        if not rest:
-            return
-        for t in reversed(choices(rest)):
+        cols = share(g, p)
+        block = held_in[k].at[:, :, cols]
+        remote(block, block, rs_sem.at[g, p, k, 0], rr_sem.at[g, p, k], x=xo).wait_recv()
+        for t in reversed(choices(rest)) if rest else ():
             spot = sum((bits[a][0] if a not in t else 1 - bits[a][0]) * 2**i for i, a in enumerate(rest))
             i = place(p, t)
-            part[i, :, columns[p]] = (
-                part[i, :, columns[p]].astype(jnp.float32)
-                + held_in[k][spot, :, columns[p]].astype(jnp.float32)
+            part[i, :, cols] = (
+                part[i, :, cols].astype(jnp.float32) + held_in[k][spot, :, cols].astype(jnp.float32)
             ).astype(jnp.bfloat16)
-
+        if not rest:
+            out_ref[:, cols] = (
+                hidden[:, cols].astype(jnp.float32)
+                + part[cube, :, cols].astype(jnp.float32)
+                + held_in[k][0, :, cols].astype(jnp.float32)
+            ).astype(jnp.bfloat16)
+
+    for g in range(halves):
+        down_fill(g)
+        for p in range(3):
+            def contract(i, _):
+                weights = wd[:, :, share(g, p)].reshape(nc * quarter, cuts[p + 1] - cuts[p])
+                made = jnp.dot(hb[lanes(i, rows), :], weights, preferred_element_type=jnp.float32)
+                part[pl.ds(group * i, group), :, share(g, p)] = made.astype(jnp.bfloat16).reshape(group, own_rows, -1)
+                return 0
+
+            lax.fori_loop(0, blocks // group, contract, 0)
+            reduce_send(g, p, 0, start)
+        for p in range(3):
+            reduce_take(g, p, 0)
+            reduce_send(g, p, 1, start)
+        if g:
+            for p in range(3):
+                reduce_take(g - 1, p, 1)
+                reduce_send(g - 1, p, 2, start)
     for p in range(3):
-        def contract(i, _):
-            weights = wd[:, :, columns[p]].reshape(nc * quarter, columns[p].size)
-            made = jnp.dot(hb[lanes(i, rows), :], weights, preferred_element_type=jnp.float32)
-            part[pl.ds(2 * i, 2), :, columns[p]] = made.astype(jnp.bfloat16).reshape(2, own_rows, columns[p].size)
-            return 0
-
-        lax.fori_loop(0, blocks // 2, contract, 0)
-        reduce_send(p, 0, start)
-    for k in range(2):
+        reduce_take(halves - 1, p, 1)
+        reduce_send(halves - 1, p, 2, start)
+    for g in range(halves):
         for p in range(3):
-            reduce_take(p, k)
-            reduce_send(p, k + 1, start)
-    for p in range(3):
-        reduce_take(p, 2)
-        cols = columns[p]
-        out_ref[:, cols] = (
-            hidden[:, cols].astype(jnp.float32)
-            + part[cube, :, cols].astype(jnp.float32)
-            + r3[0, :, cols].astype(jnp.float32)
-        ).astype(jnp.bfloat16)
+            reduce_take(g, p, 2)
 
     swap(sent)
 
     def settle(j, _):
-        zz, _off = nearest(j // nx, z, nz)
-        flow(slot(zz, lax.rem(x + lax.rem(j, nx), nx)), zz, sent)
+        zz, s = turn(j)
+        flow(s, zz, sent)
         return 0
 
     lax.fori_loop(0, nz * nx, settle, 0)
-    for j in range(1, nz * nx):
-        gate_up(j, sent)
-        downward(j, sent)
+    aside(sent)
+    for to in near + far:
+        gate_up(to, sent)
+        downward(to, sent)
     spread(sent)
-    for p in range(3):
-        for k in range(3):
-            gather(p, k, sent)
-            reduce_send(p, k, sent)
+    lend(sent)
+    for p in range(2):
+        for h in range(2):
+            for k in range(2):
+                gather(h, p, k, sent)
+    for k in range(3):
+        for p in range(3):
+            for g in range(halves):
+                reduce_send(g, p, k, sent)
+    for g in range(halves):
+        down_on(g, sent)
 
     def passed(s, _):
-        block = wgu.at[c, :, lanes(s, depth), :]
-        remote(block, block, gp_sem.at[s], gq_sem.at[s], c=co).wait_send()
-        block = wd.at[c, :, lanes(s, depth)]
-        remote(block, block, dp_sem.at[s], dq_sem.at[s], c=co).wait_send()
+        pass_on(s, sent)
         return 0
 
     lax.fori_loop(0, nz * nx, passed, 0)
-
-
-GATE_STEPS = (2, 3, 4, 5, 6, 7, 7)
 
 
 def layer(
@@ -763,12 +875,14 @@
             bf16(nx, tokens, wide), bf16(own_rows, w_out.shape[0]),
             bf16(*w_out.shape), bf16(own_rows, width), bf16(own_rows, width),
             bf16(8, own_rows, width), bf16(nc, 2, width, quarter), bf16(nc, quarter, width),
+            bf16(2, depth, quarter), bf16(quarter, depth),
             bf16(8 * own_rows, nc * quarter), bf16(8, own_rows, width),
             bf16(4, own_rows, width), bf16(2, own_rows, width), bf16(1, own_rows, width),
             dma((2,)), dma((2,)), dma((n,)), dma((n,)), dma((n,)),
-            dma((n, 2)), dma((n,)), dma((n,)), dma((n,)), dma((n,)), dma((n,)), dma((n,)), dma((n,)),
-            dma((nx * ny * nc,)), dma((nx * ny * nc,)), dma((5,)),
-            dma((3, 3, 4)), dma((3, 3)), dma((3, 3, 4)), dma((3, 3)),
+            dma((nz // 2, 2, nx, 2)), dma((n,)), dma((n,)), dma((n,)),
+            dma((nz // 2, 2, nx)), dma((n,)), dma((nz // 2,)), dma((nz // 2,)),
+            dma((2, 3)), dma((2,)), dma((nx * ny * nc,)), dma((nx * ny * nc,)), dma((5,)),
+            dma((2,)), dma((2, 2, 2, 2)), dma((2, 2, 2)), dma((nz // 2, 3, 3, 4)), dma((nz // 2, 3, 3)),
         ],
         compiler_params=pltpu.CompilerParams(
             collective_id=2, has_side_effects=True, vmem_limit_bytes=62 * 1024 * 1024

time: 219 us -> 185 us (0.84); the launches traced: 218 us -> 182 us
  Pallas kernels: 215 us -> 179 us
    pallas_call x1, Pallas kernels: 215 us -> 179 us  [layer(): pl.pallas_call(functools.partial(layer_kernel, nz, nx, ny, nc), out_shape...]
where the time goes in v2:
time: 185 us; the launch traced here: 182 us
  Pallas kernels  179 us (97%)
  local copies, waits for them, and re-layouts  3.27 us (2%)
    pallas_call x1, Pallas kernels, layer(): pl.pallas_call(functools.partial(layer_kernel, nz, nx, ny, nc), out_shape...  179 us

profile of v2, /device:TPU:20, one launch (start us, length us, event | category | flops | bytes accessed | tf_op | source)
XLA Modules:
  0.0 181.9 jit_solution(7554446474188503094)
XLA Ops:
  0.0 1.4 copy.12.gain_ref
  1.4 178.6 %layer.1 = bf16[128,2048]{1,0:T(8,128)(2,1)} custom-call(f32[2]{0:T(128)} %lam_ref.1, bf16[512,256]{1,0:T(8,128)(2,1)} %q_ref.1, bf16[512,256]{1,0:T(8,128)(2,1)} %k_ref.1, bf16[512,256]{1,0:T(8,128)(2,1)} %v_ref.1, f32[128,1]{1,0:T(8,128)} %copy.12.gain_ref, f32[1,2048]{1,0:T(1,128)} %bitcast.2, bf16[512,2048]{1,0:T(8,128)(2,1)} %res_ref.1, ...), custom_call_target="tpu_custom_call" | custom-call | tf_op jit(solution)/shard_map/layer/pallas_call | solution.py:867
  180.0 1.9 %copy.14 = bf16[128,2048]{1,0:T(8,128)(2,1)} copy(bf16[128,2048]{1,0:T(8,128)(2,1)} %layer.1) | data formatting | bytes 1048576

commit v3 on v2

--- a/solution.py
+++ b/solution.py
@@ -370,12 +370,15 @@
     return (hidden_own.astype(jnp.float32) + ffn_out).astype(jnp.bfloat16)
 
 
+FIRST = 3
+
+
 def layer_kernel(
     nz, nx, ny, nc,
     lam_ref, q_ref, k_ref, v_ref, gain_ref, norm_ref, res_ref, wout_ref, wg_ref, wu_ref, wd_ref,
     out_ref,
     q_all, qm, kv, vt, m_ref, l_ref, acc, ho, hg, wout, res, hidden, xs, wgu, wd, stage, stage_d, hb, part, r1, r2, r3,
-    q_sem, kx_sem, up_sem, low_sem, kv_sem,
+    q_sem, qo_sem, qr_sem, kx_sem, kf_sem, kv_sem,
     gs_sem, gr_sem, gp_sem, gq_sem, ds_sem, dr_sem, dp_sem, dq_sem,
     wx_sem, st_sem, hs_sem, hr_sem, in_sem, xz_sem, xs_sem, xr_sem, rs_sem, rr_sem,
 ):
@@ -413,6 +416,7 @@
         dict(x=lax.rem(x + b, nx), y=lax.rem(y + e, ny), c=lax.rem(c + f, nc))
         for b in range(nx) for e in range(ny) for f in range(nc) if e + f
     ]
+    peers += [dict(p, z=z + 1 - 2 * z0) for p in peers if "y" in p]
     for to in peers:
         pl.semaphore_signal(barrier, inc=1, device_id={**here, **to}, device_id_type=pl.DeviceIdType.MESH)
     pl.semaphore_wait(barrier, len(peers))
@@ -430,33 +434,31 @@
         go(remote(k_ref.at[:, lanes(xo, wide)], kv.at[mine, 0], kx_sem.at[0], kv_sem.at[mine], x=xo))
         go(remote(v_ref.at[:, lanes(xo, wide)], kv.at[mine, 1], kx_sem.at[1], kv_sem.at[mine], x=xo))
 
-    def up_down(zz, go_up, go_low):
-        @pl.when(jnp.logical_and(zz <= z, z < nz - 1))
-        def _():
-            go_up(jnp.minimum(z + 1, nz - 1))
-
-        @pl.when(jnp.logical_and(zz >= z, z > 0))
-        def _():
-            go_low(jnp.maximum(z - 1, 0))
-
-    def own_flow(sem, to):
-        for i, ref in enumerate((k_ref, v_ref)):
-            remote(ref.at[:, lanes(x, wide)], kv.at[mine, i], sem.at[mine], kv_sem.at[mine], z=to).start()
-
-    def flow(s, zz, go):
-        up_down(
-            zz,
-            lambda to: go(remote(kv.at[s], kv.at[s], up_sem.at[s], kv_sem.at[s], z=to)),
-            lambda to: go(remote(kv.at[s], kv.at[s], low_sem.at[s], kv_sem.at[s], z=to)),
-        )
+    halves = nz // 2
+    inner = z0 == jnp.where(z < nz // 2, 1, 0)
+    outer = jnp.logical_not(inner)
+
+    def half(g):
+        return lax.rem(z // 2 + g, halves)
+
+    def flow(e, g, go):
+        s = slot(z, lax.rem(x + e, nx))
+        zd = 2 * half(g) + jnp.where(2 * half(g) < nz // 2, 1, 0)
+        if e or go is sent:
+            go(remote(kv.at[s], kv.at[s], kf_sem.at[g, e], kv_sem.at[s], z=zd))
+        else:
+            for i, ref in enumerate((k_ref, v_ref)):
+                go(remote(ref.at[:, lanes(x, wide)], kv.at[s, i], kf_sem.at[g, e], kv_sem.at[s], z=zd))
+
+    def ask(e, go):
+        src = q_all.at[xo] if e else q_ref.at[:, lanes(x, wide)]
+        go(remote(src, q_all.at[nx + (xo if e else x)], qo_sem.at[e], qr_sem.at[xo if e else x], z=z + 1 - 2 * z0))
+
+    def swapped():
+        remote(kv.at[slot(z, xo)], kv.at[slot(z, xo)], kx_sem.at[0], kv_sem.at[slot(z, xo)], x=xo).wait_recv()
 
     def offset(q):
         return pl.multiple_of(jnp.minimum(q * quarter, units - quarter), 128)
-
-    halves = nz // 2
-
-    def half(g):
-        return lax.rem(z // 2 + g, halves)
 
     near = [(0, 1, b) for b in range(nx)]
     far = [(g, t, b) for b in range(nx) for g in range(1, halves) for t in range(2)]
@@ -490,16 +492,13 @@
         zd = half(g) * 2 + lax.rem(z0 + t, 2)
         go(remote(src, wd.at[c, :, cols], ds_sem.at[g, t, b], dr_sem.at[s], z=zd))
 
-    def aside_came():
+    def aside_came(last):
         rows = lanes(slot(z, xo), depth)
-        for block, sem in (
-            (wgu.at[c, :, rows, :], gr_sem.at[slot(z, xo)]), (stage, st_sem.at[0]),
-            (wd.at[c, :, rows], dr_sem.at[slot(z, xo)]), (stage_d, st_sem.at[1]),
-        ):
+        early = (wgu.at[c, :, rows, :], gr_sem.at[slot(z, xo)]), (stage, st_sem.at[0])
+        late = (wd.at[c, :, rows], dr_sem.at[slot(z, xo)]), (stage_d, st_sem.at[1])
+        for block, sem in late if last else early:
             remote(block, block, wx_sem.at[0, 0], sem, x=xo).wait_recv()
 
-    inner = z0 == jnp.where(z < nz // 2, 1, 0)
-    outer = jnp.logical_not(inner)
     q_me = x * 2 + z0
     own_weights = [
         pltpu.make_async_copy(ref.at[:, pl.ds(offset(q_me), quarter)], wgu.at[c, i, lanes(mine, depth), :], in_sem.at[2 + i])
@@ -510,44 +509,70 @@
     )
 
     swap(start)
-    up_down(z, lambda to: own_flow(up_sem, to), lambda to: own_flow(low_sem, to))
-    aside(start)
+
+    @pl.when(outer)
+    def _():
+        ask(0, start)
+        flow(0, 0, start)
+
+    @pl.when(inner)
+    def _():
+        for g in range(1, halves):
+            flow(0, g, start)
+
     for copy in own_weights:
         copy.start()
 
-    kv[mine, 0] = k_ref[:, lanes(x, wide)]
-    kv[mine, 1] = v_ref[:, lanes(x, wide)]
-    q_all[x] = q_ref[:, lanes(x, wide)]
-    m_ref[...] = jnp.full_like(m_ref, -jnp.inf)
-    l_ref[...] = jnp.zeros_like(l_ref)
-    acc[...] = jnp.zeros_like(acc)
-
     remote(q_all.at[x], q_all.at[xo], q_sem.at[0], q_sem.at[1], x=xo).wait_recv()
-    first_map = lax.broadcasted_iota(jnp.int32, (tokens, 2 * HD), 1) < HD
-    for h in range(nx):
-        q = q_all[h].astype(jnp.float32) * HD**-0.5
-        qm[2 * h] = jnp.where(first_map, q, 0.0).astype(jnp.bfloat16)
-        qm[2 * h + 1] = jnp.where(first_map, 0.0, q).astype(jnp.bfloat16)
-
-    def attend(s):
+
+    @pl.when(outer)
+    def _():
+        ask(1, start)
+
+    swapped()
+    aside(start)
+
+    @pl.when(inner)
+    def _():
+        for g in range(1, halves):
+            flow(1, g, start)
+
+    @pl.when(outer)
+    def _():
+        flow(1, 0, start)
+        for e in range(nx):
+            for g in range(1, halves):
+                flow(e, g, start)
+        for g in range(halves):
+            for e in range(nx):
+                flow(e, g, sent)
+        for n, to in enumerate(far[:FIRST]):
+            if n == len(far) // 2:
+                aside_came(False)
+            gate_up(to, start)
+            gate_up(to, sent)
+
+    def attend(s, low, high):
         vt[...] = kv[s, 1].astype(jnp.float32).T.astype(jnp.bfloat16)
 
-        def one(i, _):
-            scores = lax.dot_general(
-                kv[s, 0], qm[i], (((1,), (1,)), ((), ())), preferred_element_type=jnp.float32
-            )
-            old = m_ref[i]
-            high = jnp.maximum(old, jnp.max(scores, axis=0, keepdims=True))
-            shrink = jnp.exp(old - high)
-            weights = jnp.exp(scores - high)
-            l_ref[i] = l_ref[i] * shrink + jnp.sum(weights, axis=0, keepdims=True)
-            m_ref[i] = high
-            acc[i] = acc[i] * shrink + jnp.dot(
-                vt[...], weights.astype(jnp.bfloat16), preferred_element_type=jnp.float32
-            )
+        def pair(h, _):
+            both = [2 * h, 2 * h + 1]
+            scores = [
+                lax.dot_general(kv[s, 0], qm[i], (((1,), (1,)), ((), ())), preferred_element_type=jnp.float32)
+                for i in both
+            ]
+            olds = [m_ref[i] for i in both]
+            highs = [jnp.maximum(o, jnp.max(t, axis=0, keepdims=True)) for o, t in zip(olds, scores)]
+            weights = [jnp.exp(t - g) for t, g in zip(scores, highs)]
+            mixed = [jnp.dot(vt[...], w.astype(jnp.bfloat16), preferred_element_type=jnp.float32) for w in weights]
+            for i, o, g, w, t in zip(both, olds, highs, weights, mixed):
+                shrink = jnp.exp(o - g)
+                l_ref[i] = l_ref[i] * shrink + jnp.sum(w, axis=0, keepdims=True)
+                m_ref[i] = g
+                acc[i] = acc[i] * shrink + t
             return 0
 
-        lax.fori_loop(0, 2 * nx, one, 0)
+        lax.fori_loop(low, high, pair, 0)
 
     def turn(j):
         mixed = jnp.logical_and(j >= nx, j < 3 * nx) if nz > 2 else False
@@ -556,68 +581,101 @@
         zz, _off = nearest(k, z, nz)
         return zz, slot(zz, lax.rem(x + e, nx))
 
-    def step(j, _):
+    def ready(low):
+        for h in range(low, low + nx):
+            q = q_all[h].astype(jnp.float32) * HD**-0.5
+            qm[2 * h] = jnp.where(first_map, q, 0.0).astype(jnp.bfloat16)
+            qm[2 * h + 1] = jnp.where(first_map, 0.0, q).astype(jnp.bfloat16)
+
+    first_map = lax.broadcasted_iota(jnp.int32, (tokens, 2 * HD), 1) < HD
+
+    def step(n, _):
+        j = jnp.where(n < 2 * nx, lax.rem(n, nx), n - nx)
         zz, s = turn(j)
 
-        @pl.when(j > 0)
+        @pl.when(n == nx)
+        def _():
+            for e in range(nx):
+                remote(q_all.at[0], q_all.at[0], qo_sem.at[0], qr_sem.at[e], x=xo).wait_recv()
+            ready(nx)
+
+        @pl.when(zz != z)
         def _():
             remote(kv.at[s], kv.at[s], kx_sem.at[0], kv_sem.at[s], x=xo).wait_recv()
-            flow(s, zz, start)
-
-        def issue(at, where, some):
-            @pl.when(jnp.logical_and(where, j == min(at, nz * nx - 1)))
+
+        def issue(at, some):
+            @pl.when(j == min(at, nz * nx - 1))
             def _():
                 for to in some:
                     gate_up(to, start)
 
-        issue(2, outer, [to for to in far if to[1:] == (0, 0)])
+        issue(2, near[:1])
+        issue(3, [to for to in far if to[1:] == (1, 0)])
+        issue(4, [to for to in far if to[1:] == (0, 0)])
 
         @pl.when(j == min(5, nz * nx - 1))
         def _():
-            aside_came()
-
-        issue(5, outer, [to for to in far if to[1:] == (0, 1)])
-        issue(5, inner, [to for to in far if to[1:] == (1, 0)])
-        issue(5, outer, [to for to in far if to[1] == 1])
-        issue(7, inner, [to for to in far if to[1:] == (1, 1)])
-        attend(s)
+            aside_came(False)
+
+        issue(5, near[1:])
+        issue(5, [to for to in far if to[1:] == (1, 1)])
+        issue(6, [to for to in far if to[1:] == (0, 1)])
+        attend(s, jnp.where(jnp.logical_and(n >= nx, n < 2 * nx), nx, 0), jnp.where(n < nx, nx, 2 * nx))
         return 0
-
-    lax.fori_loop(0, nz * nx, step, 0)
-
-    for h in range(nx):
-        first = acc[2 * h] / l_ref[2 * h]
-        second = acc[2 * h + 1] / l_ref[2 * h + 1]
-        differ = first - lam_ref[x] * second
-        scale = lax.rsqrt(jnp.mean(differ * differ, axis=0, keepdims=True) + 1e-05)
-        ho[h] = (differ * scale * gain_ref[...]).T.astype(jnp.bfloat16)
 
     head = tp * nx + x
     me = (x * ny + y) * nc + c
 
     def spread(go):
-        n = 0
         for b in range(nx):
             for e in range(ny):
                 for f in range(nc):
-                    if b + e + f:
-                        xd, yd, cd = lax.rem(x + b, nx), lax.rem(y + e, ny), lax.rem(c + f, nc)
-                        src = ho.at[xd, lanes(yd * nc + cd, own_rows), :]
-                        go(remote(src, hg.at[:, lanes(head, wide)], hs_sem.at[n], hr_sem.at[me], x=xd, y=yd, c=cd))
-                        n += 1
-
-    spread(start)
-    hg[:, lanes(head, wide)] = ho[x, lanes(tp, own_rows), :]
+                    xd, yd, cd = lax.rem(x + b, nx), lax.rem(y + e, ny), lax.rem(c + f, nc)
+                    for p in range(0 if b + e + f else 1, 2):
+                        n = ((b * ny + e) * nc + f) * 2 + p
+                        src = ho.at[p * nx + xd, lanes(yd * nc + cd, own_rows), :]
+                        zd = z + p * (1 - 2 * z0)
+                        go(remote(src, hg.at[:, lanes(head, wide)], hs_sem.at[n], hr_sem.at[me], z=zd, x=xd, y=yd, c=cd))
+
+    @pl.when(inner)
+    def _():
+        kv[mine, 0] = k_ref[:, lanes(x, wide)]
+        kv[mine, 1] = v_ref[:, lanes(x, wide)]
+        q_all[x] = q_ref[:, lanes(x, wide)]
+        m_ref[...] = jnp.full_like(m_ref, -jnp.inf)
+        l_ref[...] = jnp.zeros_like(l_ref)
+        acc[...] = jnp.zeros_like(acc)
+        ready(0)
+        lax.fori_loop(0, nz * nx + nx, step, 0)
+
+        def finish(h, _):
+            first = acc[2 * h] / l_ref[2 * h]
+            second = acc[2 * h + 1] / l_ref[2 * h + 1]
+            differ = first - lam_ref[x] * second
+            scale = lax.rsqrt(jnp.mean(differ * differ, axis=0, keepdims=True) + 1e-05)
+            ho[h] = (differ * scale * gain_ref[...]).T.astype(jnp.bfloat16)
+            return 0
+
+        lax.fori_loop(0, 2 * nx, finish, 0)
+        spread(start)
+        hg[:, lanes(head, wide)] = ho[x, lanes(tp, own_rows), :]
+
     for copy in local_in:
         copy.wait()
     for b in range(nx):
         for e in range(ny):
             for f in range(nc):
+                xd, yd, cd = lax.rem(x + b, nx), lax.rem(y + e, ny), lax.rem(c + f, nc)
+                other = (xd * ny + yd) * nc + cd
+                block = hg.at[:, lanes((yd * nc + cd) * nx + xd, wide)]
+
+                def came():
+                    remote(block, block, hs_sem.at[0], hr_sem.at[other], x=xo).wait_recv()
+
                 if b + e + f:
-                    xd, yd, cd = lax.rem(x + b, nx), lax.rem(y + e, ny), lax.rem(c + f, nc)
-                    other = (xd * ny + yd) * nc + cd
-                    block = hg.at[:, lanes((yd * nc + cd) * nx + xd, wide)]
-                    remote(block, block, hs_sem.at[0], hr_sem.at[other], x=xo).wait_recv()
+                    came()
+                else:
+                    pl.when(outer)(came)
 
     state = res[...].astype(jnp.float32) + jnp.dot(hg[...], wout[...], preferred_element_type=jnp.float32)
     hidden[...] = state.astype(jnp.bfloat16)
@@ -638,8 +696,9 @@
 
     over = cube + flip("z")
 
-    def lend(go):
-        go(remote(xs.at[cube], xs.at[cube], xz_sem.at[0], xz_sem.at[1], **across["z"]))
+    def lend(p, go):
+        block = xs.at[cube, :, columns[p]]
+        go(remote(block, block, xz_sem.at[p, 0], xz_sem.at[p, 1], **across["z"]))
 
     def gather(h, p, k, go):
         held = [(cube, over)[h]]
@@ -653,32 +712,39 @@
         block = xs.at[pl.ds(0, 2**k), :, columns[p]]
         remote(block, block, xs_sem.at[h, p, k, 0], xr_sem.at[h, p, k], x=xo).wait_recv()
 
-    lend(start)
     for p in range(2):
+        lend(p, start)
         gather(0, p, 0, start)
-    for to in near:
-        gate_up(to, start)
+
+    @pl.when(outer)
+    def _():
+        if FIRST <= len(far) // 2:
+            aside_came(False)
+        for to in far[FIRST:] + near:
+            gate_up(to, start)
+
     for p in range(2):
         gathered(0, p, 0)
         gather(0, p, 1, start)
-
-    @pl.when(inner)
-    def _():
-        for to in far:
-            if to[1] == 0:
-                gate_up(to, start)
-
-    remote(xs.at[over], xs.at[over], xz_sem.at[0], xz_sem.at[1], x=xo).wait_recv()
     for p in range(2):
+        block = xs.at[over, :, columns[p]]
+        remote(block, block, xz_sem.at[p, 0], xz_sem.at[p, 1], x=xo).wait_recv()
         gather(1, p, 0, start)
     for p in range(2):
         gathered(1, p, 0)
         gather(1, p, 1, start)
+    aside_came(True)
 
     @pl.when(outer)
     def _():
-        for to in near:
+        for to in near + [to for to in far if to[1] == 0]:
             downward(to, start)
+
+    @pl.when(inner)
+    def _():
+        for to in far:
+            if to[1]:
+                downward(to, start)
 
     for copy in own_weights:
         copy.wait()
@@ -723,13 +789,17 @@
             hb[lanes(i, rows), cc * quarter : (cc + 1) * quarter] = jnp.where(keep, made, 0.0).astype(jnp.bfloat16)
         return 0
 
+    @pl.when(outer)
+    def _():
+        for to in far:
+            if to[1]:
+                downward(to, start)
+
     @pl.when(inner)
     def _():
-        for to in near:
+        for to in near + [to for to in far if to[1] == 0]:
             downward(to, start)
 
-    for to in far:
-        downward(to, start)
     lax.fori_loop(0, blocks // group, expand, 0)
     def place(p, flips):
         return cube + sum(flip(axis) for axis in flips)
@@ -741,13 +811,15 @@
         return sets
 
     held_in = (r1, r2, r3)
-    orders = (("x", "y", "z"), ("y", "z", "x"), ("z", "x", "y"))
+    spare_z = (("x", "y", "z"), ("y", "x", "z"))
+    even = (("x", "y", "z"), ("y", "z", "x"), ("z", "x", "y"))
+    orders = [even if g == halves - 1 else spare_z for g in range(halves)]
     span = width // halves
     tiles = span // 128
-    cuts = [0] + [128 * ((tiles * (i + 1) + 2) // 3) for i in range(3)]
+    cuts = [[0] + [128 * ((tiles * (i + 1) + len(o) - 1) // len(o)) for i in range(len(o))] for o in orders]
 
     def share(g, p):
-        return pl.ds(pl.multiple_of(half(g) * span + cuts[p], 128), cuts[p + 1] - cuts[p])
+        return pl.ds(pl.multiple_of(half(g) * span + cuts[g][p], 128), cuts[g][p + 1] - cuts[g][p])
 
     def down_on(g, go):
         block = wd.at[c, :, lanes(half(g), span)]
@@ -767,7 +839,7 @@
         remote(block, block, dp_sem.at[g], dq_sem.at[g], c=co).wait_recv()
 
     def reduce_send(g, p, k, go):
-        axis, rest = orders[p][k], orders[p][k + 1 :]
+        axis, rest = orders[g][p][k], orders[g][p][k + 1 :]
         for n, t in enumerate(choices(rest)):
             spot = sum((bits[a][0] if a not in t else 1 - bits[a][0]) * 2**i for i, a in enumerate(rest))
             src = part.at[place(p, t + (axis,)), :, share(g, p)]
@@ -775,7 +847,7 @@
             go(remote(src, dst, rs_sem.at[g, p, k, n], rr_sem.at[g, p, k], **across[axis]))
 
     def reduce_take(g, p, k):
-        axis, rest = orders[p][k], orders[p][k + 1 :]
+        axis, rest = orders[g][p][k], orders[g][p][k + 1 :]
         cols = share(g, p)
         block = held_in[k].at[:, :, cols]
         remote(block, block, rs_sem.at[g, p, k, 0], rr_sem.at[g, p, k], x=xo).wait_recv()
@@ -794,50 +866,63 @@
 
     for g in range(halves):
         down_fill(g)
-        for p in range(3):
+        for p in range(len(orders[g])):
             def contract(i, _):
-                weights = wd[:, :, share(g, p)].reshape(nc * quarter, cuts[p + 1] - cuts[p])
+                weights = wd[:, :, share(g, p)].reshape(nc * quarter, cuts[g][p + 1] - cuts[g][p])
                 made = jnp.dot(hb[lanes(i, rows), :], weights, preferred_element_type=jnp.float32)
                 part[pl.ds(group * i, group), :, share(g, p)] = made.astype(jnp.bfloat16).reshape(group, own_rows, -1)
                 return 0
 
             lax.fori_loop(0, blocks // group, contract, 0)
             reduce_send(g, p, 0, start)
-        for p in range(3):
+        for p in range(len(orders[g])):
             reduce_take(g, p, 0)
             reduce_send(g, p, 1, start)
         if g:
-            for p in range(3):
+            for p in range(len(orders[g - 1])):
                 reduce_take(g - 1, p, 1)
                 reduce_send(g - 1, p, 2, start)
-    for p in range(3):
+    for p in range(len(orders[halves - 1])):
         reduce_take(halves - 1, p, 1)
         reduce_send(halves - 1, p, 2, start)
     for g in range(halves):
-        for p in range(3):
+        for p in range(len(orders[g])):
             reduce_take(g, p, 2)
 
     swap(sent)
 
-    def settle(j, _):
-        zz, s = turn(j)
-        flow(s, zz, sent)
-        return 0
-
-    lax.fori_loop(0, nz * nx, settle, 0)
+    @pl.when(outer)
+    def _():
+        for e in range(nx):
+            ask(e, sent)
+
+    @pl.when(inner)
+    def _():
+        for e in range(nx):
+            for g in range(1, halves):
+                flow(e, g, sent)
+        for to in far:
+            gate_up(to, sent)
+        spread(sent)
+
     aside(sent)
+    @pl.when(outer)
+    def _():
+        for to in far[FIRST:]:
+            gate_up(to, sent)
+
+    for to in near:
+        gate_up(to, sent)
     for to in near + far:
-        gate_up(to, sent)
         downward(to, sent)
-    spread(sent)
-    lend(sent)
     for p in range(2):
+        lend(p, sent)
         for h in range(2):
             for k in range(2):
                 gather(h, p, k, sent)
     for k in range(3):
-        for p in range(3):
-            for g in range(halves):
+        for g in range(halves):
+            for p in range(len(orders[g])):
                 reduce_send(g, p, k, sent)
     for g in range(halves):
         down_on(g, sent)
@@ -870,19 +955,19 @@
         in_specs=[pl.BlockSpec(memory_space=pltpu.SMEM)] + [vmem] * 5 + [hbm] * 5,
         out_specs=vmem,
         scratch_shapes=[
-            bf16(nx, tokens, wide), bf16(2 * nx, tokens, wide), bf16(n, 2, tokens, wide), bf16(wide, tokens),
-            f32(2 * nx, 1, tokens), f32(2 * nx, 1, tokens), f32(2 * nx, wide, tokens),
-            bf16(nx, tokens, wide), bf16(own_rows, w_out.shape[0]),
+            bf16(2 * nx, tokens, wide), bf16(4 * nx, tokens, wide), bf16(n, 2, tokens, wide), bf16(wide, tokens),
+            f32(4 * nx, 1, tokens), f32(4 * nx, 1, tokens), f32(4 * nx, wide, tokens),
+            bf16(2 * nx, tokens, wide), bf16(own_rows, w_out.shape[0]),
             bf16(*w_out.shape), bf16(own_rows, width), bf16(own_rows, width),
             bf16(8, own_rows, width), bf16(nc, 2, width, quarter), bf16(nc, quarter, width),
             bf16(2, depth, quarter), bf16(quarter, depth),
             bf16(8 * own_rows, nc * quarter), bf16(8, own_rows, width),
             bf16(4, own_rows, width), bf16(2, own_rows, width), bf16(1, own_rows, width),
-            dma((2,)), dma((2,)), dma((n,)), dma((n,)), dma((n,)),
+            dma((2,)), dma((nx,)), dma((nx,)), dma((2,)), dma((nz // 2, nx)), dma((n,)),
             dma((nz // 2, 2, nx, 2)), dma((n,)), dma((n,)), dma((n,)),
             dma((nz // 2, 2, nx)), dma((n,)), dma((nz // 2,)), dma((nz // 2,)),
-            dma((2, 3)), dma((2,)), dma((nx * ny * nc,)), dma((nx * ny * nc,)), dma((5,)),
-            dma((2,)), dma((2, 2, 2, 2)), dma((2, 2, 2)), dma((nz // 2, 3, 3, 4)), dma((nz // 2, 3, 3)),
+            dma((2, 3)), dma((2,)), dma((2 * nx * ny * nc,)), dma((nx * ny * nc,)), dma((5,)),
+            dma((2, 2)), dma((2, 2, 2, 2)), dma((2, 2, 2)), dma((nz // 2, 3, 3, 4)), dma((nz // 2, 3, 3)),
         ],
         compiler_params=pltpu.CompilerParams(
             collective_id=2, has_side_effects=True, vmem_limit_bytes=62 * 1024 * 1024

time: 185 us -> 174 us (0.941)
  Pallas kernels: 179 us -> 168 us
    pallas_call x1, Pallas kernels: 179 us -> 168 us  [layer(): pl.pallas_call(functools.partial(layer_kernel, nz, nx, ny, nc), out_shape...]
where the time goes in v3:
time: 174 us; the launch traced here: 171 us
  Pallas kernels  168 us (97%)
  local copies, waits for them, and re-layouts  3.27 us (2%)
    pallas_call x1, Pallas kernels, layer(): pl.pallas_call(functools.partial(layer_kernel, nz, nx, ny, nc), out_shape...  168 us

profile of v3, /device:TPU:20, one launch (start us, length us, event | category | flops | bytes accessed | tf_op | source)
XLA Modules:
  0.0 171.3 jit_solution(10744375192869839740)
XLA Ops:
  0.0 1.4 copy.12.gain_ref
  1.4 168.0 %layer.1 = bf16[128,2048]{1,0:T(8,128)(2,1)} custom-call(f32[2]{0:T(128)} %lam_ref.1, bf16[512,256]{1,0:T(8,128)(2,1)} %q_ref.1, bf16[512,256]{1,0:T(8,128)(2,1)} %k_ref.1, bf16[512,256]{1,0:T(8,128)(2,1)} %v_ref.1, f32[128,1]{1,0:T(8,128)} %copy.12.gain_ref, f32[1,2048]{1,0:T(1,128)} %bitcast.2, bf16[512,2048]{1,0:T(8,128)(2,1)} %res_ref.1, ...), custom_call_target="tpu_custom_call" | custom-call | tf_op jit(solution)/shard_map/layer/pallas_call | solution.py:952
  169.4 1.9 %copy.14 = bf16[128,2048]{1,0:T(8,128)(2,1)} copy(bf16[128,2048]{1,0:T(8,128)(2,1)} %layer.1) | data formatting | bytes 1048576

commit v4 on v3

--- a/solution.py
+++ b/solution.py
@@ -370,7 +370,7 @@
     return (hidden_own.astype(jnp.float32) + ffn_out).astype(jnp.bfloat16)
 
 
-FIRST = 3
+FIRST = 2
 
 
 def layer_kernel(
@@ -450,6 +450,14 @@
             for i, ref in enumerate((k_ref, v_ref)):
                 go(remote(ref.at[:, lanes(x, wide)], kv.at[s, i], kf_sem.at[g, e], kv_sem.at[s], z=zd))
 
+    def relay(e, go):
+        s = slot(z + 1 - 2 * z0, lax.rem(x + e, nx))
+        if go is start:
+            remote(kv.at[s], kv.at[s], kx_sem.at[0], kv_sem.at[s], x=xo).wait_recv()
+        for g in range(1, halves):
+            zd = 2 * half(g) + jnp.where(2 * half(g) < nz // 2, 1, 0)
+            go(remote(kv.at[s], kv.at[s], kf_sem.at[g, nx + e], kv_sem.at[s], z=zd))
+
     def ask(e, go):
         src = q_all.at[xo] if e else q_ref.at[:, lanes(x, wide)]
         go(remote(src, q_all.at[nx + (xo if e else x)], qo_sem.at[e], qr_sem.at[xo if e else x], z=z + 1 - 2 * z0))
@@ -541,13 +549,9 @@
     def _():
         flow(1, 0, start)
         for e in range(nx):
-            for g in range(1, halves):
-                flow(e, g, start)
-        for g in range(halves):
-            for e in range(nx):
-                flow(e, g, sent)
-        for n, to in enumerate(far[:FIRST]):
-            if n == len(far) // 2:
+            flow(e, 0, sent)
+        for to in near + far[:FIRST]:
+            if to == near[1]:
                 aside_came(False)
             gate_up(to, start)
             gate_up(to, sent)
@@ -599,7 +603,12 @@
                 remote(q_all.at[0], q_all.at[0], qo_sem.at[0], qr_sem.at[e], x=xo).wait_recv()
             ready(nx)
 
-        @pl.when(zz != z)
+        for e in range(nx):
+            @pl.when(n == nx + e)
+            def _():
+                relay(e, start)
+
+        @pl.when(zz // 2 != z // 2)
         def _():
             remote(kv.at[s], kv.at[s], kx_sem.at[0], kv_sem.at[s], x=xo).wait_recv()
 
@@ -610,16 +619,20 @@
                     gate_up(to, start)
 
         issue(2, near[:1])
-        issue(3, [to for to in far if to[1:] == (1, 0)])
-        issue(4, [to for to in far if to[1:] == (0, 0)])
+
+        @pl.when(j == min(4, nz * nx - 1))
+        def _():
+            for e in range(nx):
+                relay(e, sent)
+
+        issue(4, [to for to in far if to[1:] == (1, 0)])
 
         @pl.when(j == min(5, nz * nx - 1))
         def _():
             aside_came(False)
 
         issue(5, near[1:])
-        issue(5, [to for to in far if to[1:] == (1, 1)])
-        issue(6, [to for to in far if to[1:] == (0, 1)])
+        issue(6, [to for to in far if to[1:] == (1, 1)])
         attend(s, jnp.where(jnp.logical_and(n >= nx, n < 2 * nx), nx, 0), jnp.where(n < nx, nx, 2 * nx))
         return 0
 
@@ -718,14 +731,19 @@
 
     @pl.when(outer)
     def _():
-        if FIRST <= len(far) // 2:
-            aside_came(False)
-        for to in far[FIRST:] + near:
+        for to in far[FIRST:]:
             gate_up(to, start)
 
     for p in range(2):
         gathered(0, p, 0)
         gather(0, p, 1, start)
+
+    @pl.when(inner)
+    def _():
+        for to in far:
+            if to[1] == 0:
+                gate_up(to, start)
+
     for p in range(2):
         block = xs.at[over, :, columns[p]]
         remote(block, block, xz_sem.at[p, 0], xz_sem.at[p, 1], x=xo).wait_recv()
@@ -733,28 +751,12 @@
     for p in range(2):
         gathered(1, p, 0)
         gather(1, p, 1, start)
-    aside_came(True)
-
-    @pl.when(outer)
-    def _():
-        for to in near + [to for to in far if to[1] == 0]:
-            downward(to, start)
-
-    @pl.when(inner)
-    def _():
-        for to in far:
-            if to[1]:
-                downward(to, start)
-
-    for copy in own_weights:
-        copy.wait()
-
     def pass_on(s, go):
         block = wgu.at[c, :, lanes(s, depth), :]
         go(remote(block, block, gp_sem.at[s], gq_sem.at[s], c=co))
 
     def fill(j, _):
-        s = lax.rem(half(0) * 2 * nx + j, nz * nx)
+        s = lax.rem(z * nx + jnp.where(z < nz // 2, j, nx - 1 - j + nz * nx), nz * nx)
 
         @pl.when(s // nx != z)
         def _():
@@ -769,7 +771,31 @@
         remote(block, block, gp_sem.at[s], gq_sem.at[s], c=co).wait_recv()
         return 0
 
+    aside_came(True)
+
+    @pl.when(outer)
+    def _():
+        for to in far[FIRST:]:
+            gate_up(to, sent)
+        for to in near + [to for to in far if to[1] == 0] + [to for to in far if to[1]]:
+            downward(to, start)
+
+    @pl.when(inner)
+    def _():
+        for to in far:
+            if to[1]:
+                downward(to, start)
+
+    for copy in own_weights:
+        copy.wait()
     lax.fori_loop(0, nz * nx, fill, 0)
+    @pl.when(inner)
+    def _():
+        for to in near + far:
+            gate_up(to, sent)
+        for to in near + [to for to in far if to[1] == 0]:
+            downward(to, start)
+
     lax.fori_loop(0, nz * nx, filled, 0)
     for h in range(2):
         for p in range(2):
@@ -789,17 +815,6 @@
             hb[lanes(i, rows), cc * quarter : (cc + 1) * quarter] = jnp.where(keep, made, 0.0).astype(jnp.bfloat16)
         return 0
 
-    @pl.when(outer)
-    def _():
-        for to in far:
-            if to[1]:
-                downward(to, start)
-
-    @pl.when(inner)
-    def _():
-        for to in near + [to for to in far if to[1] == 0]:
-            downward(to, start)
-
     lax.fori_loop(0, blocks // group, expand, 0)
     def place(p, flips):
         return cube + sum(flip(axis) for axis in flips)
@@ -821,22 +836,30 @@
     def share(g, p):
         return pl.ds(pl.multiple_of(half(g) * span + cuts[g][p], 128), cuts[g][p + 1] - cuts[g][p])
 
-    def down_on(g, go):
-        block = wd.at[c, :, lanes(half(g), span)]
-        go(remote(block, block, dp_sem.at[g], dq_sem.at[g], c=co))
+    def down_on(s, go):
+        block = wd.at[c, :, lanes(s, depth)]
+        go(remote(block, block, dp_sem.at[s], dq_sem.at[s], c=co))
 
     def down_fill(g):
-        for n in range(2 * nx):
+        def one(n, _):
             s = half(g) * 2 * nx + n
 
             @pl.when(s // nx != z)
             def _():
                 block = wd.at[c, :, lanes(s, depth)]
-                remote(block, block, dp_sem.at[g], dr_sem.at[s], c=co).wait_recv()
-
-        down_on(g, start)
-        block = wd.at[co, :, lanes(half(g), span)]
-        remote(block, block, dp_sem.at[g], dq_sem.at[g], c=co).wait_recv()
+                remote(block, block, dp_sem.at[s], dr_sem.at[s], c=co).wait_recv()
+
+            down_on(s, start)
+            return 0
+
+        def other(n, _):
+            s = half(g) * 2 * nx + n
+            block = wd.at[co, :, lanes(s, depth)]
+            remote(block, block, dp_sem.at[s], dq_sem.at[s], c=co).wait_recv()
+            return 0
+
+        lax.fori_loop(0, 2 * nx, one, 0)
+        lax.fori_loop(0, 2 * nx, other, 0)
 
     def reduce_send(g, p, k, go):
         axis, rest = orders[g][p][k], orders[g][p][k + 1 :]
@@ -901,18 +924,9 @@
         for e in range(nx):
             for g in range(1, halves):
                 flow(e, g, sent)
-        for to in far:
-            gate_up(to, sent)
         spread(sent)
 
     aside(sent)
-    @pl.when(outer)
-    def _():
-        for to in far[FIRST:]:
-            gate_up(to, sent)
-
-    for to in near:
-        gate_up(to, sent)
     for to in near + far:
         downward(to, sent)
     for p in range(2):
@@ -924,11 +938,10 @@
         for g in range(halves):
             for p in range(len(orders[g])):
                 reduce_send(g, p, k, sent)
-    for g in range(halves):
-        down_on(g, sent)
 
     def passed(s, _):
         pass_on(s, sent)
+        down_on(s, sent)
         return 0
 
     lax.fori_loop(0, nz * nx, passed, 0)
@@ -963,9 +976,9 @@
             bf16(2, depth, quarter), bf16(quarter, depth),
             bf16(8 * own_rows, nc * quarter), bf16(8, own_rows, width),
             bf16(4, own_rows, width), bf16(2, own_rows, width), bf16(1, own_rows, width),
-            dma((2,)), dma((nx,)), dma((nx,)), dma((2,)), dma((nz // 2, nx)), dma((n,)),
+            dma((2,)), dma((nx,)), dma((nx,)), dma((2,)), dma((nz // 2, 2 * nx)), dma((n,)),
             dma((nz // 2, 2, nx, 2)), dma((n,)), dma((n,)), dma((n,)),
-            dma((nz // 2, 2, nx)), dma((n,)), dma((nz // 2,)), dma((nz // 2,)),
+            dma((nz // 2, 2, nx)), dma((n,)), dma((n,)), dma((n,)),
             dma((2, 3)), dma((2,)), dma((2 * nx * ny * nc,)), dma((nx * ny * nc,)), dma((5,)),
             dma((2, 2)), dma((2, 2, 2, 2)), dma((2, 2, 2)), dma((nz // 2, 3, 3, 4)), dma((nz // 2, 3, 3)),
         ],

time: 174 us -> 172 us (0.989)
  no operation moved by 1% of the time
where the time goes in v4:
time: 172 us; the launch traced here: 170 us
  Pallas kernels  167 us (97%)
  local copies, waits for them, and re-layouts  3.27 us (2%)
    pallas_call x1, Pallas kernels, layer(): pl.pallas_call(functools.partial(layer_kernel, nz, nx, ny, nc), out_shape...  167 us

profile of v4, /device:TPU:20, one launch (start us, length us, event | category | flops | bytes accessed | tf_op | source)
XLA Modules:
  0.0 169.8 jit_solution(9111177583498458225)
XLA Ops:
  0.0 1.4 copy.12.gain_ref
  1.4 166.5 %layer.1 = bf16[128,2048]{1,0:T(8,128)(2,1)} custom-call(f32[2]{0:T(128)} %lam_ref.1, bf16[512,256]{1,0:T(8,128)(2,1)} %q_ref.1, bf16[512,256]{1,0:T(8,128)(2,1)} %k_ref.1, bf16[512,256]{1,0:T(8,128)(2,1)} %v_ref.1, f32[128,1]{1,0:T(8,128)} %copy.12.gain_ref, f32[1,2048]{1,0:T(1,128)} %bitcast.2, bf16[512,2048]{1,0:T(8,128)(2,1)} %res_ref.1, ...), custom_call_target="tpu_custom_call" | custom-call | tf_op jit(solution)/shard_map/layer/pallas_call | solution.py:965
  167.9 1.9 %copy.14 = bf16[128,2048]{1,0:T(8,128)(2,1)} copy(bf16[128,2048]{1,0:T(8,128)(2,1)} %layer.1) | data formatting | bytes 1048576

commit v5 on v4

--- a/solution.py
+++ b/solution.py
@@ -898,13 +898,13 @@
 
             lax.fori_loop(0, blocks // group, contract, 0)
             reduce_send(g, p, 0, start)
-        for p in range(len(orders[g])):
-            reduce_take(g, p, 0)
-            reduce_send(g, p, 1, start)
         if g:
             for p in range(len(orders[g - 1])):
                 reduce_take(g - 1, p, 1)
                 reduce_send(g - 1, p, 2, start)
+        for p in range(len(orders[g])):
+            reduce_take(g, p, 0)
+            reduce_send(g, p, 1, start)
     for p in range(len(orders[halves - 1])):
         reduce_take(halves - 1, p, 1)
         reduce_send(halves - 1, p, 2, start)

time: 172 us -> 170 us (0.988)
  Pallas kernels: 167 us -> 163 us
    pallas_call x1, Pallas kernels: 167 us -> 163 us  [layer(): pl.pallas_call(functools.partial(layer_kernel, nz, nx, ny, nc), out_shape...]
where the time goes in v5:
time: 170 us; the launch traced here: 167 us
  Pallas kernels  163 us (96%)
  local copies, waits for them, and re-layouts  3.27 us (2%)
    pallas_call x1, Pallas kernels, layer(): pl.pallas_call(functools.partial(layer_kernel, nz, nx, ny, nc), out_shape...  163 us

profile of v5, /device:TPU:20, one launch (start us, length us, event | category | flops | bytes accessed | tf_op | source)
XLA Modules:
  0.0 166.6 jit_solution(14793013936287186511)
XLA Ops:
  0.0 1.4 copy.12.gain_ref
  1.4 163.4 %layer.1 = bf16[128,2048]{1,0:T(8,128)(2,1)} custom-call(f32[2]{0:T(128)} %lam_ref.1, bf16[512,256]{1,0:T(8,128)(2,1)} %q_ref.1, bf16[512,256]{1,0:T(8,128)(2,1)} %k_ref.1, bf16[512,256]{1,0:T(8,128)(2,1)} %v_ref.1, f32[128,1]{1,0:T(8,128)} %copy.12.gain_ref, f32[1,2048]{1,0:T(1,128)} %bitcast.2, bf16[512,2048]{1,0:T(8,128)(2,1)} %res_ref.1, ...), custom_call_target="tpu_custom_call" | custom-call | tf_op jit(solution)/shard_map/layer/pallas_call | solution.py:965
  164.8 1.9 %copy.14 = bf16[128,2048]{1,0:T(8,128)(2,1)} copy(bf16[128,2048]{1,0:T(8,128)(2,1)} %layer.1) | data formatting | bytes 1048576
